TPU v7x, 128 devices: a whole 4x4x4 slice. The times are simulated.
128 devices in a mesh: ep: 16 (over z, x), tp: 8 (over y, core).
Axes of the slice: x: 4, y: 4, z: 4, core: 2. Of those that a mesh axis runs over, the one named last changes fastest.
Arguments:
- tokens: bfloat16 [18432, 2048], P(('ep', 'tp')), may hold values from -6 to 6
- norm_gain: float32 [2048], replicated, may hold values from 0.1 to 1.9
- expert_ids: int32 [18432, 8], P(('ep', 'tp')), may hold values from 0 to 31, all different within a row; in each aligned block of 144 rows (0 to 143, 144 to 287, ...) at most 72 rows name the same one
- route_weights: float32 [18432, 8], P(('ep', 'tp')), may hold values from 0.3 to 1
- expert_gate: bfloat16 [32, 512, 2048], P('ep', 'tp'), may hold values from -0.125 to 0.125
- expert_up: bfloat16 [32, 512, 2048], P('ep', 'tp'), may hold values from -0.125 to 0.125
- expert_down: bfloat16 [32, 512, 2048], P('ep', 'tp'), may hold values from -0.25 to 0.25
- shared_gate: bfloat16 [512, 2048], P('tp'), may hold values from -0.125 to 0.125
- shared_up: bfloat16 [512, 2048], P('tp'), may hold values from -0.125 to 0.125
- shared_down: bfloat16 [512, 2048], P('tp'), may hold values from -0.25 to 0.25
- side_in: bfloat16 [2048, 1024], P('ep'), may hold values from -0.125 to 0.125
- side_out: bfloat16 [2048, 1024], P('ep'), may hold values from -0.1875 to 0.1875
- side_gate: bfloat16 [2048], replicated, may hold values from -0.125 to 0.125
Outputs:
- mixed: bfloat16 [18432, 2048], P(('ep', 'tp'))
Inputs may be any that keep to these rules, and one draw needn't show every extreme that they name: `expert_ids`: each row names 8 different experts of 0 to 31; within the rows of one device (aligned blocks of 144 rows) no expert is named more than 72 times, and in some of those blocks some expert is named exactly 72 times.
All inputs are finite; a program needn't handle non-finite values.
Results may differ from a plain program's by a relative error of at most 0.0068.
Values may be sent and summed in bfloat16 or wider, within the bound.
A program may use at most 320 MiB of HBM per device.

v0:
```python
import jax
import jax.numpy as jnp
from jax import lax
from jax.sharding import PartitionSpec as P

norm_eps = 1.0


def side_by_side(arrays, axis, dim, along):
    widths = [a.shape[along] for a in arrays]
    both = jnp.concatenate(arrays, axis=along)
    out = lax.all_gather(both, axis, axis=dim, tiled=True)
    return tuple(jnp.split(out, [sum(widths[:k]) for k in range(1, len(widths))], axis=along))


def normalize(tokens, norm_gain):
    values = tokens.astype(jnp.float32)
    scale_inv = lax.rsqrt(jnp.mean(values * values, axis=-1, keepdims=True) + norm_eps)
    return (values * scale_inv * norm_gain).astype(jnp.bfloat16)


def swiglu(gate_part, up_part):
    return (jax.nn.silu(gate_part) * up_part).astype(jnp.bfloat16)


def body(
    tokens,
    norm_gain,
    expert_ids,
    route_weights,
    expert_gate,
    expert_up,
    expert_down,
    shared_gate,
    shared_up,
    shared_down,
    side_in,
    side_out,
    side_gate,
):
    normed = normalize(tokens, norm_gain)
    tok_count, width = normed.shape
    top_count = expert_ids.shape[1]
    groups = lax.axis_size("ep")
    local_experts = expert_gate.shape[0]
    experts_all = groups * local_experts
    capacity = 2 * tok_count * top_count // experts_all
    pair_count = tok_count * top_count
    flat_ids = expert_ids.reshape(pair_count)
    one_hot = (flat_ids[:, None] == jnp.arange(experts_all, dtype=jnp.int32)[None, :]).astype(
        jnp.int32
    )
    earlier = jnp.cumsum(one_hot, axis=0) - 1
    slot_of = jnp.sum(one_hot * earlier, axis=1)
    position = flat_ids * capacity + slot_of
    source_row = jnp.arange(pair_count, dtype=jnp.int32) // top_count
    buffers = (
        jnp.zeros((experts_all * capacity, width), jnp.bfloat16)
        .at[position]
        .set(normed[source_row])
    )
    buffers = buffers.reshape(groups, local_experts, capacity, width)
    received = lax.all_to_all(buffers, "ep", split_axis=0, concat_axis=0, tiled=True)
    gate_piece, up_piece, down_piece = side_by_side(
        (expert_gate, expert_up, expert_down), "tp", 1, 0
    )
    gate_part = jnp.einsum(
        "secd,efd->secf", received, gate_piece, preferred_element_type=jnp.float32
    )
    up_part = jnp.einsum("secd,efd->secf", received, up_piece, preferred_element_type=jnp.float32)
    hidden = swiglu(gate_part, up_part)
    total = jnp.einsum("secf,efd->secd", hidden, down_piece, preferred_element_type=jnp.float32)
    returned = lax.all_to_all(
        total.astype(jnp.bfloat16), "ep", split_axis=0, concat_axis=0, tiled=True
    )
    picked = returned.reshape(experts_all * capacity, width)[position]
    weighted = picked.astype(jnp.float32) * route_weights.reshape(pair_count, 1)
    routed = jnp.sum(weighted.reshape(tok_count, top_count, width), axis=1)
    gate_piece, up_piece, down_piece = side_by_side(
        (shared_gate, shared_up, shared_down), "tp", 0, 1
    )
    gate_part = jnp.einsum("td,fd->tf", normed, gate_piece, preferred_element_type=jnp.float32)
    up_part = jnp.einsum("td,fd->tf", normed, up_piece, preferred_element_type=jnp.float32)
    hidden = swiglu(gate_part, up_part)
    shared = jnp.dot(hidden, down_piece, preferred_element_type=jnp.float32)
    whole_in, whole_out = side_by_side((side_in, side_out), "ep", 0, 1)
    side_hidden = jax.nn.silu(jnp.dot(normed, whole_in, preferred_element_type=jnp.float32)).astype(
        jnp.bfloat16
    )
    side_value = jnp.einsum("ts,ds->td", side_hidden, whole_out, preferred_element_type=jnp.float32)
    opening = jax.nn.sigmoid(jnp.dot(normed, side_gate, preferred_element_type=jnp.float32))
    return (routed + shared + opening[:, None] * side_value).astype(jnp.bfloat16)


def solution(mesh):
    placed = (
        P(("ep", "tp"), None),
        P(),
        P(("ep", "tp"), None),
        P(("ep", "tp"), None),
        P("ep", "tp", None),
        P("ep", "tp", None),
        P("ep", "tp", None),
        P("tp", None),
        P("tp", None),
        P("tp", None),
        P("ep", None),
        P("ep", None),
        P(),
    )
    return jax.shard_map(
        body, mesh=mesh, in_specs=placed, out_specs=P(("ep", "tp"), None), check_vma=False
    )
```

profile of v0, /device:TPU:1, one launch (start us, length us, event | category | flops | bytes accessed | tf_op | source)
XLA Modules:
  0.0 421.9 jit_solution(12502017451172172665)
XLA Ops:
  6.5 0.0 copy-start.7
  6.6 0.0 all-gather.4.cloned.1.call-start
  6.6 2.8 pad_maximum_fusion
  9.4 0.0 all-gather.4.cloned.1.call-update
  9.4 0.0 all-gather.6.cloned.1.call-start
  9.5 0.0 copy-done.3
  9.5 0.0 copy-done.2
  9.5 0.0 copy-done.1
  9.5 0.9 pad_maximum_fusion.1
  10.5 0.0 all-gather.6.cloned.1.call-update
  10.5 0.0 copy-done.6
  10.5 0.1 copy.24
  10.6 0.1 eq.29
  10.7 0.1 eq.25
  10.8 9.1 %reduce-window.6 = s32[32,9,128]{2,1,0:T(8,128)S(1)} reduce-window(s32[32,9,128]{2,1,0:T(8,128)S(1)} %fusion.49, s32[]{:T(128)} %constant.38.clone.1), window={size=1x1x128 pad=0_0x0_0x127_0}, to_apply=%region_0.0 | reduce-window | flops 4681728 | bytes 294916 | tf_op jit(solution)/shard_map/reduce-window
  19.9 0.1 slice.12
  20.1 0.2 copy.26
  20.3 0.1 copy.27
  20.4 0.1 copy.23
  20.5 0.1 mul.75
  20.6 0.1 add_add_fusion
  20.8 0.1 fusion.51
  20.9 0.0 copy-done
  20.9 0.2 fusion.28
  21.1 0.2 fusion.30
  21.3 35.8 %scatter_custom_fusion = bf16[2304,2048]{1,0:T(8,128)(2,1)} fusion(s32[1152]{0:T(1024)S(1)} %fusion.53, bf16[144,2048]{1,0:T(8,128)(2,1)S(1)} %fusion.30, s32[2048]{0:T(1024)S(1)} %pad_clamp_fusion.1, bf16[]{:T(256)} %constant.36.clone.1), kind=kCustom, calls=%fused_computation.17 | custom fusion | bytes 9437186 | tf_op jit(solution)/shard_map/scatter | solution.py:60
  57.1 0.0 copy-start.4
  57.1 0.0 copy-start.5
  57.1 8.6 %all-to-all-start = ((bf16[16,2,72,2048]{3,2,1,0:T(8,128)(2,1)}), bf16[16,2,72,2048]{3,2,1,0:T(8,128)(2,1)}, u32[]{:S(2)}, u32[]{:S(2)}) async-start(bf16[16,2,72,2048]{3,2,1,0:T(8,128)(2,1)} %bitcast.63), calls=%async_computation | async-start | bytes 18874368 | tf_op jit(solution)/shard_map/all_to_all | solution.py:63
  65.7 0.0 all-gather.8.cloned.1.call-start
  65.8 0.8 pad_maximum_fusion.2
  66.6 0.0 all-gather.8.cloned.1.call-update
  66.6 141.8 %all-to-all-done = bf16[16,2,72,2048]{3,2,1,0:T(8,128)(2,1)} async-done(((bf16[16,2,72,2048]{3,2,1,0:T(8,128)(2,1)}), bf16[16,2,72,2048]{3,2,1,0:T(8,128)(2,1)}, u32[]{:S(2)}, u32[]{:S(2)}) %all-to-all-start) | async-done | bytes 9437216 | tf_op jit(solution)/shard_map/all_to_all | solution.py:63
  208.5 8.9 %fusion.1 = f32[2,512,16,72]{1,3,2,0:T(8,128)S(1)} fusion(bf16[16,2,72,2048]{3,2,1,0:T(8,128)(2,1)} %all-to-all-done, bf16[6,512,2048]{2,1,0:T(8,128)(2,1)} %all-gather.4.cloned.1.call-done), kind=kOutput, calls=%fused_computation.6 | convolution fusion | flops 4831838208 | bytes 18350080 | tf_op jit(solution)/shard_map/secd,efd->secf/dot_general | solution.py:70
  217.4 9.6 %fusion.5 = bf16[16,2,72,512]{3,2,0,1:T(8,128)(2,1)S(1)} fusion(f32[2,512,16,72]{1,3,2,0:T(8,128)S(1)} %fusion.1, bf16[16,2,72,2048]{3,2,1,0:T(8,128)(2,1)} %all-to-all-done, bf16[6,512,2048]{2,1,0:T(8,128)(2,1)} %all-gather.4.cloned.1.call-done), kind=kOutput, calls=%fused_computation.11 | convolution fusion | flops 4838916096 | bytes 20709376 | tf_op jit(solution)/shard_map/secd,efd->secf/dot_general | solution.py:67
  227.0 9.7 %convert_bitcast_fusion = bf16[16,2,72,2048]{3,2,0,1:T(8,128)(2,1)} fusion(bf16[16,2,72,512]{3,2,0,1:T(8,128)(2,1)S(1)} %fusion.5, bf16[6,512,2048]{2,1,0:T(8,128)(2,1)} %all-gather.4.cloned.1.call-done), kind=kOutput, calls=%fused_computation.5 | convolution fusion | flops 4836556800 | bytes 15990784 | tf_op jit(solution)/shard_map/secf,efd->secd/dot_general | solution.py:72
  236.7 9.4 %copy.30 = bf16[16,2,72,2048]{3,2,1,0:T(8,128)(2,1)} copy(bf16[16,2,72,2048]{3,2,0,1:T(8,128)(2,1)} %convert_bitcast_fusion) | data formatting | bytes 18874368 | tf_op jit(solution)/shard_map/convert_element_type | solution.py:74
  246.2 5.2 %all-to-all-start.1 = ((bf16[16,2,72,2048]{3,2,1,0:T(8,128)(2,1)}), bf16[16,2,72,2048]{3,2,1,0:T(8,128)(2,1)}, u32[]{:S(2)}, u32[]{:S(2)}) async-start(bf16[16,2,72,2048]{3,2,1,0:T(8,128)(2,1)} %copy.30), calls=%async_computation.1 | async-start | bytes 18874368 | tf_op jit(solution)/shard_map/all_to_all | solution.py:73
  251.4 0.1 copy.31
  251.5 0.3 fusion.57
  251.8 0.0 all-gather.6.cloned.1.call-done
  251.8 2.4 fusion.26
  254.2 0.0 all-gather.8.cloned.1.call-done
  254.3 6.7 %fusion.19 = f32[144,2048]{1,0:T(8,128)} fusion(bf16[2048,2048]{1,0:T(8,128)(2,1)} %all-gather.8.cloned.1.call-done, bf16[144,2048]{1,0:T(8,128)(2,1)S(1)} %fusion.30, f32[144]{0:T(256)S(1)} %add_divide_fusion), kind=kOutput, calls=%fused_computation.29 | convolution fusion | flops 1208991744 | bytes 10158656 | tf_op jit(solution)/shard_map/ts,ds->td/dot_general | solution.py:90
  261.0 126.8 %all-to-all-done.1 = bf16[16,2,72,2048]{3,2,1,0:T(8,128)(2,1)} async-done(((bf16[16,2,72,2048]{3,2,1,0:T(8,128)(2,1)}), bf16[16,2,72,2048]{3,2,1,0:T(8,128)(2,1)}, u32[]{:S(2)}, u32[]{:S(2)}) %all-to-all-start.1) | async-done | bytes 9437216 | tf_op jit(solution)/shard_map/all_to_all | solution.py:73
  387.7 15.5 %gather_fusion = bf16[1152,2048]{1,0:T(8,128)(2,1)} fusion(bf16[2304,2048]{1,0:T(8,128)(2,1)} %bitcast.12, s32[2048]{0:T(1024)S(1)} %pad_clamp_fusion), kind=kCustom, calls=%fused_computation.1 | custom fusion | bytes 9441792 | tf_op jit(solution)/shard_map/gather | solution.py:76
  403.3 7.0 %fusion = f32[144,2048]{1,0:T(8,128)S(1)} fusion(bf16[1152,2048]{1,0:T(8,128)(2,1)} %gather_fusion, f32[144,8]{1,0:T(8,128)S(1)} %copy.31), kind=kLoop, calls=%fused_computation.4 | loop fusion | flops 6782976 | bytes 5902848 | tf_op jit(solution)/shard_map/reduce_sum | solution.py:78
  410.3 4.6 %fusion.22 = bf16[144,2048]{1,0:T(8,128)(2,1)} fusion(f32[144,2048]{1,0:T(8,128)} %fusion.19, f32[144,2048]{1,0:T(8,128)S(1)} %fusion, bf16[512,6144]{1,0:T(8,128)(2,1)} %all-gather.6.cloned.1.call-done, bf16[144,2048]{1,0:T(8,128)(2,1)S(1)} %fusion.30, f32[144,512]{1,0:T(8,128)S(1)} %fusion.26), kind=kOutput, calls=%fused_computation.30 | convolution fusion | flops 605306880 | bytes 8028160 | tf_op jit(solution)/shard_map/dot_general | solution.py:85
  (23 shorter events, 0.2 us)
Async XLA Ops:
  6.5 2.9 copy-start.3
  6.5 2.9 copy-start.2
  6.5 3.0 copy-start.1
  6.5 3.9 copy-start.6
  6.5 14.3 %copy-start = (bf16[144,2048]{1,0:T(8,128)(2,1)S(1)}, bf16[144,2048]{1,0:T(8,128)(2,1)}, u32[]{:S(2)}) copy-start(bf16[144,2048]{1,0:T(8,128)(2,1)} %param.13) | copy-start | bytes 1769476
  6.5 14.6 %copy-start.7 = (f32[2048]{0:T(1024)S(1)}, f32[2048]{0:T(1024)}, u32[]{:S(2)}) copy-start(f32[2048]{0:T(1024)} %param.14) | copy-start | bytes 24580
  6.6 201.9 %all-gather.4.cloned.1.call-start = ((), (), s32[]{:S(2)}) async-start(), calls=%async_computation.2 | async-start | bytes 14155776 | tf_op jit(solution)/shard_map/all_gather | solution.py:12
  9.4 242.4 %all-gather.6.cloned.1.call-start = ((), (), s32[]{:S(2)}) async-start(), calls=%async_computation.3 | async-start | bytes 7077888 | tf_op jit(solution)/shard_map/all_gather | solution.py:12
  57.1 8.7 %copy-start.4 = (bf16[128,1024]{1,0:T(8,128)(2,1)S(1)}, bf16[128,1024]{1,0:T(8,128)(2,1)}, u32[]{:S(2)}) copy-start(bf16[128,1024]{1,0:T(8,128)(2,1)} %param.24) | copy-start | bytes 786436
  57.1 8.7 %copy-start.5 = (bf16[128,1024]{1,0:T(8,128)(2,1)S(1)}, bf16[128,1024]{1,0:T(8,128)(2,1)}, u32[]{:S(2)}) copy-start(bf16[128,1024]{1,0:T(8,128)(2,1)} %param.23) | copy-start | bytes 786436
  57.1 151.4 %all-to-all-start = ((bf16[16,2,72,2048]{3,2,1,0:T(8,128)(2,1)}), bf16[16,2,72,2048]{3,2,1,0:T(8,128)(2,1)}, u32[]{:S(2)}, u32[]{:S(2)}) async-start(bf16[16,2,72,2048]{3,2,1,0:T(8,128)(2,1)} %bitcast.63), calls=%async_computation | async-start | bytes 18874368 | tf_op jit(solution)/shard_map/all_to_all | solution.py:63
  65.7 188.5 %all-gather.8.cloned.1.call-start = ((), (), s32[]{:S(2)}) async-start(), calls=%async_computation.4 | async-start | bytes 8912896 | tf_op jit(solution)/shard_map/all_gather | solution.py:12
  246.2 5.2 %copy-start.8 = (f32[144,8]{0,1:T(8,128)S(1)}, f32[144,8]{0,1:T(8,128)}, u32[]{:S(2)}) copy-start(f32[144,8]{0,1:T(8,128)} %param.16) | copy-start | bytes 13828
  246.2 5.3 %copy-start.9 = (bf16[2048]{0:T(1024)(128)(2,1)S(1)}, bf16[2048]{0:T(1024)(128)(2,1)}, u32[]{:S(2)}) copy-start(bf16[2048]{0:T(1024)(128)(2,1)} %param.25) | copy-start | bytes 12292
  246.2 141.6 %all-to-all-start.1 = ((bf16[16,2,72,2048]{3,2,1,0:T(8,128)(2,1)}), bf16[16,2,72,2048]{3,2,1,0:T(8,128)(2,1)}, u32[]{:S(2)}, u32[]{:S(2)}) async-start(bf16[16,2,72,2048]{3,2,1,0:T(8,128)(2,1)} %copy.30), calls=%async_computation.1 | async-start | bytes 18874368 | tf_op jit(solution)/shard_map/all_to_all | solution.py:73
Sparse Core Ops, SparseCore 0:
  9.5 70.8 all-gather.3
  82.2 41.2 all-gather.5
  125.6 127.8 all-gather.7
where the time goes:
time: 427 us; the launch traced here: 422 us
  waiting for transfers between devices  269 us (63%)
  local copies, waits for them, and re-layouts  61.8 us (14%)
  matrix products  42.3 us (10%)
  other arithmetic  21.4 us (5%)
  starting transfers between devices  13.9 us (3%)
  between operations  13.8 us (3%)
    all_to_all x1, waiting for transfers between devices, body(): lax.all_to_all(buffers, 'ep', split_axis=0, concat_axis=0, tiled=True)  142 us
    all_to_all x1, waiting for transfers between devices, body(): lax.all_to_all(total.astype(jnp.bfloat16), 'ep', split_axis=0, concat_axi...  127 us
    scatter x1, local copies, waits for them, and re-layouts, body(): buffers = jnp.zeros((experts_all * capacity, width), jnp.bfloat16).at[pos...  35.8 us
    gather x1, local copies, waits for them, and re-layouts, body(): picked = returned.reshape(experts_all * capacity, width)[position]  15.5 us
    dot_general x1, matrix products, body(): jnp.einsum('secf,efd->secd', hidden, down_piece, preferred_element_type=j...  9.69 us
    dot_general x1, matrix products, body(): jnp.einsum('secd,efd->secf', received, gate_piece, preferred_element_type...  9.63 us
    convert_element_type x1, local copies, waits for them, and re-layouts, body(): total.astype(jnp.bfloat16)  9.45 us
    another operation x2, other arithmetic  9.11 us
  transfers between devices with their start and end apart: 5, of which 2 were waited for; matrix products, arithmetic and copies ran while one was open for 23% of the time, Pallas kernels for 0%

commit v1 on v0

v1 whole, which is shorter than its diff:
```python
import functools

import jax
import jax.numpy as jnp
from jax import lax
from jax.experimental import pallas as pl
from jax.experimental.pallas import tpu as pltpu
from jax.sharding import PartitionSpec as P

norm_eps = 1.0
TOK = 144
D = 2048
HALF = 1024
SUB = 512
GROUP = 4
ROWS = GROUP * TOK

ORDER = [
    (2, 2), (2, 1), (2, 3), (2, 0),
    (1, 2), (1, 1), (3, 2), (3, 1),
    (1, 3), (1, 0), (3, 3), (3, 0),
    (0, 2), (0, 1), (0, 3), (0, 0),
]
SLOT = {place: i for i, place in enumerate(ORDER)}
DY = [0, 1, 3, 2]
DYI = {dy: i for i, dy in enumerate(DY)}
NT = (((1,), (1,)), ((), ()))


def kernel(
    tok_ref, gain_ref, w8_ref, gate_hbm, up_hbm, down_hbm, shared_hbm, side_hbm, sgate_ref,
    out_ref,
    xs, wg, wu, wd, wx, wdx, sb, sh, hid, rl, rf, rl2, rf2, wrow, wpat,
    ag_send, ag_m1, ag_f1, ag_m2, ag_f2,
    w_send, w_recv, w_fsend, w_frecv, w_dsend, w_drecv, w_loc,
    x_send, x_recv, x_loc, sb_dsend, sb_drecv, sh_send, sh_recv, sh_dsend, sh_drecv, sh_loc,
    rs_send, rl_sem, rf_sem, rl2_sem, rf2_sem,
):
    ep = lax.axis_index("ep")
    tp = lax.axis_index("tp")
    z, x = ep // 4, ep % 4
    y, core = tp // 2, tp % 2

    def at_ep(dz, dx):
        return (((z + dz) % 4) * 4 + (x + dx) % 4, tp)

    def at_y(dy):
        return (ep, ((y + dy) % 4) * 2 + core)

    partner = (ep, tp + 1 - 2 * core)

    def along(axis, step):
        return at_ep(step, 0) if axis == "z" else at_ep(0, step)

    def remote(src, dst, send, recv, where):
        return pltpu.make_async_remote_copy(
            src_ref=src, dst_ref=dst, send_sem=send, recv_sem=recv, device_id=where,
            device_id_type=pl.DeviceIdType.MESH,
        )

    wx[pl.ds(96, 32), :] = jnp.zeros((32, D), jnp.bfloat16)
    wx[pl.ds(128, 16), :] = sgate_ref[...]
    wx[pl.ds(144, 48), :] = jnp.zeros((48, D), jnp.bfloat16)
    wx[pl.ds(224, 32), :] = jnp.zeros((32, D), jnp.bfloat16)
    wdx[pl.ds(96, 32), :] = jnp.zeros((32, D), jnp.bfloat16)

    barrier = pltpu.get_barrier_semaphore()
    peers = [at_ep(*p) for p in ORDER if p != (0, 0)] + [at_y(d) for d in (1, 2, 3)] + [partner]
    for peer in peers:
        pl.semaphore_signal(barrier, inc=1, device_id=peer, device_id_type=pl.DeviceIdType.MESH)
    pl.semaphore_wait(barrier, len(peers))

    big = [(gate_hbm, wg), (up_hbm, wu), (down_hbm, wd)]
    w_p, w_m, w_fp, w_fm, w_d, w_l = [], [], [], [], {}, []
    for i, (src, dst) in enumerate(big):
        w_p.append(remote(src, dst.at[2 * DYI[3]], w_send.at[i, 0], w_recv.at[i, 0], at_y(1)))
        w_m.append(remote(src, dst.at[2 * DYI[1]], w_send.at[i, 1], w_recv.at[i, 1], at_y(3)))
        w_fp.append(remote(
            dst.at[2 * DYI[3], pl.ds(0, 64)], dst.at[2 * DYI[2], pl.ds(0, 64)],
            w_fsend.at[i, 0], w_frecv.at[i, 0], at_y(1)))
        w_fm.append(remote(
            dst.at[2 * DYI[1], pl.ds(64, 64)], dst.at[2 * DYI[2], pl.ds(64, 64)],
            w_fsend.at[i, 1], w_frecv.at[i, 1], at_y(3)))
        for dy in DY:
            w_d[i, dy] = remote(
                src if dy == 0 else dst.at[2 * DYI[dy]], dst.at[2 * DYI[dy] + 1],
                w_dsend.at[i, dy], w_drecv.at[i, dy], partner)
        w_l.append(pltpu.make_async_copy(src, dst.at[0], w_loc.at[i]))
    for i in range(3):
        w_p[i].start()
        w_m[i].start()
    for i in range(3):
        w_d[i, 0].start()
        w_l[i].start()

    values = tok_ref[...].astype(jnp.float32)
    scale_inv = lax.rsqrt(jnp.mean(values * values, axis=-1, keepdims=True) + norm_eps)
    normed = (values * scale_inv * gain_ref[...]).astype(jnp.bfloat16)
    xs[0, SLOT[0, 0]] = normed[:, :HALF]
    xs[1, SLOT[0, 0]] = normed[:, HALF:]

    axes = [("x", "z"), ("z", "x")]

    def src_slot(h, d1, d2):
        return SLOT[(d2, d1) if h == 0 else (d1, d2)]

    lo, hi = pl.ds(0, SUB), pl.ds(SUB, SUB)
    m1, f1, m2, f2 = {}, {}, {}, {}
    for h in range(2):
        a1, a2 = axes[h]
        s = functools.partial(src_slot, h)
        m1[h, 0] = remote(xs.at[h, s(0, 0)], xs.at[h, s(3, 0)], ag_send.at[h], ag_m1.at[h, 0], along(a1, 1))
        m1[h, 1] = remote(xs.at[h, s(0, 0)], xs.at[h, s(1, 0)], ag_send.at[h], ag_m1.at[h, 1], along(a1, 3))
        f1[h, 0] = remote(
            xs.at[h, s(3, 0), :, lo], xs.at[h, s(2, 0), :, lo], ag_send.at[h], ag_f1.at[h, 0], along(a1, 1))
        f1[h, 1] = remote(
            xs.at[h, s(1, 0), :, hi], xs.at[h, s(2, 0), :, hi], ag_send.at[h], ag_f1.at[h, 1], along(a1, 3))
        for d in range(4):
            m2[h, d, 0] = remote(
                xs.at[h, s(d, 0)], xs.at[h, s(d, 3)], ag_send.at[h], ag_m2.at[h, d, 0], along(a2, 1))
            m2[h, d, 1] = remote(
                xs.at[h, s(d, 0)], xs.at[h, s(d, 1)], ag_send.at[h], ag_m2.at[h, d, 1], along(a2, 3))
            f2[h, d, 0] = remote(
                xs.at[h, s(d, 3), :, lo], xs.at[h, s(d, 2), :, lo],
                ag_send.at[h], ag_f2.at[h, d, 0], along(a2, 1))
            f2[h, d, 1] = remote(
                xs.at[h, s(d, 1), :, hi], xs.at[h, s(d, 2), :, hi],
                ag_send.at[h], ag_f2.at[h, d, 1], along(a2, 3))

    both = [(h, k) for h in range(2) for k in range(2)]
    for h, k in both:
        m1[h, k].start()

    w_small, s_small = [], []
    for dz, dx in ORDER[:-1]:
        there = at_ep(dz, dx)
        mine = SLOT[(4 - dz) % 4, (4 - dx) % 4]
        w_small.append(remote(w8_ref.at[there[0]], wrow.at[mine], x_send.at[0], x_recv.at[0], there))
        s_small.append(remote(
            side_hbm.at[there[0]], sb.at[0, :, pl.ds(pl.multiple_of(ep * 128, 128), 128)],
            x_send.at[1], x_recv.at[1], there))
    for c in w_small + s_small:
        c.start()
    own_side = pltpu.make_async_copy(
        side_hbm.at[ep], sb.at[0, :, pl.ds(pl.multiple_of(ep * 128, 128), 128)], x_loc.at[0])
    own_side.start()
    wrow[SLOT[0, 0]] = w8_ref[ep]

    for h, k in both:
        m2[h, 0, k].start()

    owner = ep // 2
    is_src = tp == owner
    on_core = core == owner % 2
    sh_copies = [remote(shared_hbm, sh, sh_send.at[d - 1], sh_recv, at_y(d)) for d in (1, 2, 3)]
    sh_cross = remote(sh, sh, sh_dsend, sh_drecv, partner)
    sh_own = pltpu.make_async_copy(shared_hbm, sh, sh_loc)

    @pl.when(is_src)
    def _():
        for c in sh_copies:
            c.start()
        sh_own.start()
        sh_own.wait()
        sh_cross.start()

    for h, k in both:
        m1[h, k].wait_recv()
        f1[h, k].start()
    for h in range(2):
        for d in (3, 1):
            for k in range(2):
                m2[h, d, k].start()
    for h, k in both:
        m2[h, 0, k].wait_recv()
        f2[h, 0, k].start()

    pltpu.make_async_copy(wrow.at[pl.ds(0, 15)], wrow.at[pl.ds(0, 15)], x_recv.at[0]).wait()
    columns = jnp.transpose(wrow[...].reshape(128, 256))
    low_lane = lax.broadcasted_iota(jnp.int32, (TOK, 128), 1) < 64
    for i in range(16):
        wpat[i] = jnp.where(low_lane, columns[:TOK, 8 * i:8 * i + 1], columns[:TOK, 8 * i + 1:8 * i + 2])

    for h, k in both:
        f1[h, k].wait_recv()
    for h in range(2):
        for k in range(2):
            m2[h, 2, k].start()

    def weights_on(i):
        w_p[i].wait_recv()
        w_fp[i].start()
        w_d[i, 3].start()
        w_m[i].wait_recv()
        w_fm[i].start()
        w_d[i, 1].start()

    weights_on(0)
    own_side.wait()
    pltpu.make_async_copy(
        sb.at[0, :, pl.ds(0, 1920)], sb.at[0, :, pl.ds(0, 1920)], x_recv.at[1]).wait()
    sb_cross = remote(sb.at[0], sb.at[1], sb_dsend, sb_drecv, partner)
    sb_cross.start()
    for h, k in both:
        m2[h, 3, k].wait_recv()
        f2[h, 3, k].start()
    weights_on(1)
    for h, k in both:
        m2[h, 1, k].wait_recv()
        f2[h, 1, k].start()

    @pl.when(jnp.logical_and(on_core, jnp.logical_not(is_src)))
    def _():
        sh_copies[0].wait_recv()
        sh_cross.start()

    @pl.when(jnp.logical_not(on_core))
    def _():
        sh_cross.wait_recv()

    weights_on(2)
    for h, k in both:
        m2[h, 2, k].wait_recv()
        f2[h, 2, k].start()
    for i in range(3):
        w_fp[i].wait_recv()
        w_fm[i].wait_recv()
        w_d[i, 2].start()

    sb_cross.wait_recv()
    wx[pl.ds(0, 64), :] = sb[core]
    wdx[pl.ds(0, 64), :] = sb[1 - core]
    wx[pl.ds(64, 32), :] = sh[0]
    wx[pl.ds(192, 32), :] = sh[1]
    wdx[pl.ds(64, 32), :] = sh[2]

    for d in (0, 3, 1, 2):
        for h, k in both:
            f2[h, d, k].wait_recv()
    for i in range(3):
        w_l[i].wait()
        for dy in DY:
            w_d[i, dy].wait_recv()
    for h in range(2):
        pltpu.make_async_copy(xs.at[h, pl.ds(0, 15)], xs.at[h, pl.ds(0, 15)], ag_send.at[h]).wait()

    f32 = jnp.float32

    def silu(v):
        return v / (1.0 + jnp.exp(-v))

    def both_halves(xa, xb, w):
        return lax.dot_general(xa, w[:, :HALF], NT, preferred_element_type=f32) + lax.dot_general(
            xb, w[:, HALF:], NT, preferred_element_type=f32)

    def compute(group):
        base = GROUP * group
        pattern = wpat[pl.ds(base, GROUP)].reshape(ROWS, 128)

        def up_step(c, carry):
            xa = xs[0, pl.ds(base, GROUP)].reshape(ROWS, HALF)
            xb = xs[1, pl.ds(base, GROUP)].reshape(ROWS, HALF)
            rows = pl.ds(2 * c, 2)
            gate = both_halves(xa, xb, wg[rows].reshape(256, D))
            up = both_halves(xa, xb, wu[rows].reshape(256, D))
            w2 = jnp.concatenate([pattern, pattern], axis=1)
            hid[:, pl.ds(pl.multiple_of(c * 256, 256), 256)] = (silu(gate) * up * w2).astype(jnp.bfloat16)
            return carry

        lax.fori_loop(0, 4, up_step, 0)
        xa = xs[0, pl.ds(base, GROUP)].reshape(ROWS, HALF)
        xb = xs[1, pl.ds(base, GROUP)].reshape(ROWS, HALF)
        dense = both_halves(xa, xb, wx[...])
        first, second = dense[:, :128], dense[:, 128:]
        lane = lax.broadcasted_iota(jnp.int32, (ROWS, 128), 1)
        opening = 1.0 / (1.0 + jnp.exp(-second[:, :1]))
        factor = jnp.where(lane < 64, opening, second)
        hid[:, pl.ds(1024, 128)] = (silu(first) * factor).astype(jnp.bfloat16)

        def down_step(n, carry):
            h = n // 2
            cols = pl.ds(pl.multiple_of(n * SUB, SUB), SUB)
            to = pl.ds(pl.multiple_of((n % 2) * SUB, SUB), SUB)
            part = jnp.dot(hid[:, :1024], wd[:, :, cols].reshape(1024, SUB), preferred_element_type=f32)
            part = part + jnp.dot(hid[:, 1024:], wdx[:, cols], preferred_element_type=f32)
            xs[h, pl.ds(base, GROUP), :, to] = part.astype(jnp.bfloat16).reshape(GROUP, TOK, SUB)
            return carry

        lax.fori_loop(0, 4, down_step, 0)

    rs_axes = [("z", "x"), ("x", "z")]

    def dst_slot(h, d1, q):
        return SLOT[(d1, q) if h == 0 else (q, d1)]

    r1, s1, r2, s2 = {}, {}, {}, {}
    for h in range(2):
        b1, b2 = rs_axes[h]
        t = functools.partial(dst_slot, h)
        for q in range(4):
            r1[h, q, 0] = remote(
                xs.at[h, t(2, q), :, lo], rl.at[h, q, 0], rs_send.at[h], rl_sem.at[h, q, 0], along(b1, 1))
            r1[h, q, 1] = remote(
                xs.at[h, t(2, q), :, hi], rl.at[h, q, 1], rs_send.at[h], rl_sem.at[h, q, 1], along(b1, 3))
            s1[h, q, 0] = remote(
                xs.at[h, t(1, q)], rf.at[h, q, 0], rs_send.at[h], rf_sem.at[h, q, 0], along(b1, 1))
            s1[h, q, 1] = remote(
                xs.at[h, t(3, q)], rf.at[h, q, 1], rs_send.at[h], rf_sem.at[h, q, 1], along(b1, 3))
        r2[h, 0] = remote(
            xs.at[h, t(0, 2), :, lo], rl2.at[h, 0], rs_send.at[h], rl2_sem.at[h, 0], along(b2, 1))
        r2[h, 1] = remote(
            xs.at[h, t(0, 2), :, hi], rl2.at[h, 1], rs_send.at[h], rl2_sem.at[h, 1], along(b2, 3))
        s2[h, 0] = remote(xs.at[h, t(0, 1)], rf2.at[h, 0], rs_send.at[h], rf2_sem.at[h, 0], along(b2, 1))
        s2[h, 1] = remote(xs.at[h, t(0, 3)], rf2.at[h, 1], rs_send.at[h], rf2_sem.at[h, 1], along(b2, 3))

    def add(slot, h, cols, *more):
        total = xs[h, slot, :, cols].astype(f32)
        for m in more:
            total = total + m.astype(f32)
        xs[h, slot, :, cols] = total.astype(jnp.bfloat16)

    halves = [lo, hi]
    whole = pl.ds(0, HALF)

    def relay(h, q):
        for k in range(2):
            r1[h, q, k].start()

    def pass_on(h, q, k):
        r1[h, q, k].wait_recv()
        add(dst_slot(h, (1, 3)[k], q), h, halves[k], rl[h, q, k])
        s1[h, q, k].start()

    def collect(h, q):
        for k in range(2):
            s1[h, q, k].wait_recv()
        add(dst_slot(h, 0, q), h, whole, rf[h, q, 0], rf[h, q, 1])

    def relay2(h):
        for k in range(2):
            r2[h, k].start()

    def pass_on2(h, k):
        r2[h, k].wait_recv()
        add(dst_slot(h, 0, (1, 3)[k]), h, halves[k], rl2[h, k])
        s2[h, k].start()

    compute(0)
    relay(1, 2)
    for q in (2, 1, 3, 0):
        relay(0, q)
    compute(1)
    for q in (2, 1):
        pass_on(0, q, 0)
        pass_on(0, q, 1)
    for k in range(2):
        pass_on(1, 2, k)
    relay(1, 1)
    relay(1, 3)
    compute(2)
    for q in (3, 0):
        pass_on(0, q, 0)
        pass_on(0, q, 1)
    for q in (1, 3):
        for k in range(2):
            pass_on(1, q, k)
    collect(1, 2)
    relay2(1)
    compute(3)
    relay(1, 0)
    for q, k in ((1, 0), (3, 1)):
        collect(1, q)
        pass_on2(1, k)
    for k in range(2):
        pass_on(1, 0, k)
    collect(0, 2)
    relay2(0)
    for q, k in ((1, 0), (3, 1)):
        collect(0, q)
        pass_on2(0, k)
    collect(1, 0)
    collect(0, 0)
    for h in (1, 0):
        for k in range(2):
            s2[h, k].wait_recv()
        total = xs[h, SLOT[0, 0]].astype(f32) + rf2[h, 0].astype(f32) + rf2[h, 1].astype(f32)
        out_ref[:, pl.ds(h * HALF, HALF)] = total.astype(jnp.bfloat16)

    for h in range(2):
        pltpu.make_async_copy(xs.at[h, pl.ds(0, 15)], xs.at[h, pl.ds(0, 15)], rs_send.at[h]).wait()
    for i in range(3):
        w_p[i].wait_send()
        w_m[i].wait_send()
        w_fp[i].wait_send()
        w_fm[i].wait_send()
        for dy in DY:
            w_d[i, dy].wait_send()
    pltpu.make_async_copy(wrow.at[pl.ds(0, 15)], wrow.at[pl.ds(0, 15)], x_send.at[0]).wait()
    pltpu.make_async_copy(
        sb.at[0, :, pl.ds(0, 1920)], sb.at[0, :, pl.ds(0, 1920)], x_send.at[1]).wait()
    sb_cross.wait_send()

    @pl.when(is_src)
    def _():
        for c in sh_copies:
            c.wait_send()

    @pl.when(on_core)
    def _():
        sh_cross.wait_send()


def body(
    tokens, norm_gain, expert_ids, route_weights, expert_gate, expert_up, expert_down,
    shared_gate, shared_up, shared_down, side_in, side_out, side_gate,
):
    ep = lax.axis_index("ep")
    core = lax.axis_index("tp") % 2
    experts = jnp.arange(32, dtype=jnp.int32)
    chosen = expert_ids.T[None, :, :] == experts[:, None, None]
    dense = jnp.sum(jnp.where(chosen, route_weights.T[None, :, :], 0.0), axis=1)
    w8 = jnp.pad(dense.reshape(16, 2, TOK), ((0, 0), (0, 6), (0, 256 - TOK)))
    side = jnp.where(core == 0, side_in, side_out).T.reshape(16, 64, 128)
    first = (ep % 2) * 32
    shared = jnp.stack([
        lax.dynamic_slice_in_dim(a, first, 32, axis=0) for a in (shared_gate, shared_up, shared_down)
    ])
    sgate = jnp.pad(side_gate.reshape(1, D), ((0, 15), (0, 0)))
    bf16, f32 = jnp.bfloat16, jnp.float32
    dma, vmem = pltpu.SemaphoreType.DMA, pltpu.VMEM
    in_vmem = pl.BlockSpec(memory_space=pltpu.VMEM)
    in_any = pl.BlockSpec(memory_space=pl.ANY)
    return pl.pallas_call(
        kernel,
        out_shape=jax.ShapeDtypeStruct((TOK, D), bf16),
        in_specs=[in_vmem, in_vmem, in_vmem] + [in_any] * 5 + [in_vmem],
        out_specs=in_vmem,
        scratch_shapes=[
            vmem((2, 16, TOK, HALF), bf16),
            vmem((8, 128, D), bf16),
            vmem((8, 128, D), bf16),
            vmem((8, 128, D), bf16),
            vmem((256, D), bf16),
            vmem((128, D), bf16),
            vmem((2, 64, D), bf16),
            vmem((3, 32, D), bf16),
            vmem((ROWS, 1152), bf16),
            vmem((2, 4, 2, TOK, SUB), bf16),
            vmem((2, 4, 2, TOK, HALF), bf16),
            vmem((2, 2, TOK, SUB), bf16),
            vmem((2, 2, TOK, HALF), bf16),
            vmem((16, 8, 256), f32),
            vmem((16, TOK, 128), f32),
            dma((2,)), dma((2, 2)), dma((2, 2)), dma((2, 4, 2)), dma((2, 4, 2)),
            dma((3, 2)), dma((3, 2)), dma((3, 2)), dma((3, 2)), dma((3, 4)), dma((3, 4)), dma((3,)),
            dma((2,)), dma((2,)), dma((1,)), dma(()), dma(()), dma((3,)), dma(()), dma(()), dma(()), dma(()),
            dma((2,)), dma((2, 4, 2)), dma((2, 4, 2)), dma((2, 2)), dma((2, 2)),
        ],
        compiler_params=pltpu.CompilerParams(
            collective_id=0, has_side_effects=True, vmem_limit_bytes=60 * 1024 * 1024),
        name="routed_layer",
    )(
        tokens, norm_gain.reshape(1, D), w8,
        expert_gate.reshape(128, D), expert_up.reshape(128, D), expert_down.reshape(128, D),
        shared, side, sgate,
    )


def solution(mesh):
    placed = (
        P(("ep", "tp"), None),
        P(),
        P(("ep", "tp"), None),
        P(("ep", "tp"), None),
        P("ep", "tp", None),
        P("ep", "tp", None),
        P("ep", "tp", None),
        P("tp", None),
        P("tp", None),
        P("tp", None),
        P("ep", None),
        P("ep", None),
        P(),
    )
    return jax.shard_map(
        body, mesh=mesh, in_specs=placed, out_specs=P(("ep", "tp"), None), check_vma=False
    )
```

time: 427 us -> 152 us (0.36); the launches traced: 422 us -> 151 us
  waiting for transfers between devices: 269 us -> 0 us
  Pallas kernels: 0 us -> 145 us
  local copies, waits for them, and re-layouts: 61.8 us -> 5.08 us
  matrix products: 42.3 us -> 0 us
  other arithmetic: 21.4 us -> 0.91 us
  starting transfers between devices: 13.9 us -> 0 us
  between operations: 13.8 us -> 0.1 us
    all_to_all x2 -> x0, waiting for transfers between devices: 269 us -> none  [the longest x1 142 us: body(): lax.all_to_all(buffers, 'ep', split_axis=0, concat_axis=0, tiled=True)]
    pallas_call x0 -> x1, Pallas kernels: none -> 145 us  [body(): pl.pallas_call(kernel, out_shape=jax.ShapeDtypeStruct((TOK, D), bf16), in...]
    dot_general x7 -> x0, matrix products: 42.3 us -> none  [the longest x1 9.69 us: body(): jnp.einsum('secf,efd->secd', hidden, down_piece, preferred_element_type=j...]
    scatter x1 -> x0, local copies, waits for them, and re-layouts: 35.8 us -> none  [body(): buffers = jnp.zeros((experts_all * capacity, width), jnp.bfloat16).at[pos...]
    gather x1 -> x0, local copies, waits for them, and re-layouts: 15.5 us -> none  [body(): picked = returned.reshape(experts_all * capacity, width)[position]]
    all_to_all x2 -> x0, starting transfers between devices: 13.8 us -> none  [the longest x1 8.6 us: body(): lax.all_to_all(buffers, 'ep', split_axis=0, concat_axis=0, tiled=True)]
    convert_element_type x1 -> x0, local copies, waits for them, and re-layouts: 9.45 us -> none  [body(): total.astype(jnp.bfloat16)]
    another operation x2 -> x1, other arithmetic: 9.11 us -> 0.79 us  [body(): jnp.stack([lax.dynamic_slice_in_dim(a, first, 32, axis=0) for a in (share...]
  transfers between devices with their start and end apart: 5 -> 0, of which waited for: 2 -> 0; matrix products, arithmetic and copies ran while one was open for 23% -> 0% of each run, Pallas kernels for 0% -> 0%
where the time goes in v1:
time: 152 us; the launch traced here: 151 us
  Pallas kernels  145 us (95%)
  local copies, waits for them, and re-layouts  5.08 us (3%)
    pallas_call x1, Pallas kernels, body(): pl.pallas_call(kernel, out_shape=jax.ShapeDtypeStruct((TOK, D), bf16), in...  145 us

profile of v1, /device:TPU:1, one launch (start us, length us, event | category | flops | bytes accessed | tf_op | source)
XLA Modules:
  0.0 151.5 jit_solution(7010515668296177754)
XLA Ops:
  0.0 0.0 copy-start
  0.0 0.0 copy-start.7
  0.0 0.0 copy-start.6
  0.0 0.0 copy-start.5
  0.0 0.7 copy-done.7
  0.7 0.0 copy-done.6
  0.8 0.0 copy-done.5
  0.8 0.1 select_reduce_fusion
  0.9 0.0 copy-start.2
  0.9 0.0 copy-start.1
  0.9 0.6 pad.9.sgate_ref
  1.5 0.7 pad.8.w8_ref
  2.2 0.0 copy-done
  2.2 0.0 copy-done.2
  2.2 0.0 copy-done.1
  2.3 0.0 copy-start.3
  2.3 0.0 copy-start.4
  2.3 0.8 copy.15
  3.2 0.1 copy-done.3
  3.2 0.1 copy-done.4
  3.4 0.8 pad_maximum_fusion.shared_hbm
  4.1 145.4 %routed_layer.1 = bf16[144,2048]{1,0:T(8,128)(2,1)} custom-call(bf16[144,2048]{1,0:T(8,128)(2,1)} %tok_ref.1, f32[1,2048]{1,0:T(1,128)} %bitcast.19, f32[16,8,256]{2,1,0:T(8,128)} %pad.8.w8_ref, bf16[128,2048]{1,0:T(8,128)(2,1)} %bitcast.16, bf16[128,2048]{1,0:T(8,128)(2,1)} %bitcast.17, bf16[128,2048]{1,0:T(8,128)(2,1)} %bitcast.18, ...), custom_call_target="tpu_custom_call" | custom-call | tf_op jit(solution)/shard_map/routed_layer/pallas_call | solution.py:433
  149.5 1.9 %copy.17 = bf16[144,2048]{1,0:T(8,128)(2,1)} copy(bf16[144,2048]{1,0:T(8,128)(2,1)} %routed_layer.1) | data formatting | bytes 1179648
  (5 shorter events, 0.1 us)
Async XLA Ops:
  0.0 2.2 %copy-start = (bf16[64,2048]{1,0:T(8,128)(2,1)S(1)}, bf16[64,2048]{1,0:T(8,128)(2,1)}, u32[]{:S(2)}) copy-start(bf16[64,2048]{1,0:T(8,128)(2,1)} %param.20) | copy-start | bytes 786436
  0.0 0.7 copy-start.7
  0.0 0.8 copy-start.6
  0.0 0.8 copy-start.5
  0.9 1.4 copy-start.2
  0.9 1.3 copy-start.1
  2.3 1.0 copy-start.3
  2.3 1.0 copy-start.4

commit v2 on v1

--- a/solution.py
+++ b/solution.py
@@ -16,10 +16,31 @@
 ROWS = GROUP * TOK
 
 ORDER = [
-    (2, 2), (2, 1), (2, 3), (2, 0),
-    (1, 2), (1, 1), (3, 2), (3, 1),
-    (1, 3), (1, 0), (3, 3), (3, 0),
-    (0, 2), (0, 1), (0, 3), (0, 0),
+    (2, 2), (1, 2), (2, 1), (2, 3),
+    (3, 3), (3, 2), (0, 2), (2, 0),
+    (1, 1), (1, 3), (3, 1), (3, 0),
+    (1, 0), (0, 1), (0, 3), (0, 0),
+]
+GROUPS = [12, 8, 4, 0]
+PAIRS = {
+    "g3a": 0, "g3b": 2, "g2a": 4, "g2b": 6, "g1a": 8, "g1b": 10, "g0a": 12, "g0b": 14,
+}
+SUM_ORDER = [
+    ("C", "gu3a"), ("C", "g2b"), ("relay", 1, 0, 1), ("relay", 1, 0, 0), ("relay", 0, 0, 0), ("relay", 0, 0, 1),
+    ("C", "g1a"), ("free", 0, 3, 0), ("free", 1, 1, 0), ("free", 0, 1, 0), ("free", 1, 1, 1), ("C", "g2a"),
+    ("relay", 1, 3, 0), ("relay", 1, 3, 1), ("free", 0, 2, 1), ("free", 0, 3, 1), ("free", 1, 3, 1), ("C", "gu3b"),
+    ("C", "g3a"), ("relay", 1, 2, 0), ("relay", 0, 2, 1), ("relay", 0, 2, 0), ("relay", 1, 2, 1), ("relay", 1, 1, 1),
+    ("free", 0, 2, 0), ("relay", 1, 1, 0), ("C", "g3b"), ("relay", 0, 3, 1), ("relay", 0, 3, 0), ("free", 1, 2, 1),
+    ("free", 1, 2, 0), ("relay", 0, 1, 1), ("relay", 0, 1, 0), ("C", "g0a"), ("pass", 1, 3, 1), ("free", 1, 0, 0),
+    ("pass", 0, 0, 0), ("pass", 1, 0, 0), ("free", 0, 0, 0), ("C", "g1b"), ("free", 1, 3, 0), ("pass", 1, 2, 0),
+    ("pass", 0, 2, 1), ("pass", 0, 2, 0), ("pass", 1, 3, 0), ("free", 0, 1, 1), ("free", 0, 0, 1), ("pass", 0, 0, 1),
+    ("C", "g0b"), ("pass", 1, 2, 1), ("pass", 0, 3, 1), ("free", 1, 0, 1), ("pass", 1, 1, 0), ("pass", 1, 0, 1),
+    ("pass", 0, 3, 0), ("pass", 1, 1, 1), ("pass", 0, 1, 1), ("pass", 0, 1, 0), ("collect", 0, 2, 0),
+    ("relay2", 0, 0, 0), ("relay2", 0, 0, 1), ("collect", 1, 2, 0), ("relay2", 1, 0, 0), ("relay2", 1, 0, 1),
+    ("collect", 0, 0, 0), ("collect", 1, 3, 0), ("free2", 1, 0, 1), ("collect", 0, 3, 0), ("free2", 0, 0, 1),
+    ("collect", 1, 0, 0), ("collect", 1, 1, 0), ("free2", 1, 0, 0), ("collect", 0, 1, 0), ("free2", 0, 0, 0),
+    ("pass2", 0, 0, 0), ("pass2", 0, 0, 1), ("pass2", 1, 0, 0), ("pass2", 1, 0, 1), ("final", 0, 0, 0),
+    ("final", 1, 0, 0),
 ]
 SLOT = {place: i for i, place in enumerate(ORDER)}
 DY = [0, 1, 3, 2]
@@ -86,7 +107,7 @@
                 src if dy == 0 else dst.at[2 * DYI[dy]], dst.at[2 * DYI[dy] + 1],
                 w_dsend.at[i, dy], w_drecv.at[i, dy], partner)
         w_l.append(pltpu.make_async_copy(src, dst.at[0], w_loc.at[i]))
-    for i in range(3):
+    for i in range(2):
         w_p[i].start()
         w_m[i].start()
     for i in range(3):
@@ -164,6 +185,56 @@
         sh_own.wait()
         sh_cross.start()
 
+    f32 = jnp.float32
+
+    def silu(v):
+        return v / (1.0 + jnp.exp(-v))
+
+    def both_halves(xa, xb, w):
+        return lax.dot_general(xa, w[:, :HALF], NT, preferred_element_type=f32) + lax.dot_general(
+            xb, w[:, HALF:], NT, preferred_element_type=f32)
+
+    def rows_of(base):
+        return (xs[0, pl.ds(base, GROUP)].reshape(ROWS, HALF), xs[1, pl.ds(base, GROUP)].reshape(ROWS, HALF))
+
+    def hidden(base, first, count):
+        pattern = wpat[pl.ds(base, GROUP)].reshape(ROWS, 128)
+        w2 = jnp.concatenate([pattern, pattern], axis=1)
+
+        def step(c, carry):
+            xa, xb = rows_of(base)
+            rows = pl.ds(2 * c, 2)
+            gate = both_halves(xa, xb, wg[rows].reshape(256, D))
+            up = both_halves(xa, xb, wu[rows].reshape(256, D))
+            value = (silu(gate) * up * w2).astype(jnp.bfloat16)
+            hid[pl.ds(base, GROUP), :, pl.ds(pl.multiple_of(c * 256, 256), 256)] = value.reshape(GROUP, TOK, 256)
+            return carry
+
+        lax.fori_loop(first, first + count, step, 0)
+
+    def dense_hidden(base):
+        xa, xb = rows_of(base)
+        dense = both_halves(xa, xb, wx[...])
+        first, second = dense[:, :128], dense[:, 128:]
+        lane = lax.broadcasted_iota(jnp.int32, (ROWS, 128), 1)
+        opening = 1.0 / (1.0 + jnp.exp(-second[:, :1]))
+        factor = jnp.where(lane < 64, opening, second)
+        value = (silu(first) * factor).astype(jnp.bfloat16)
+        hid[pl.ds(base, GROUP), :, pl.ds(1024, 128)] = value.reshape(GROUP, TOK, 128)
+
+    def down(base):
+        def step(n, carry):
+            h = n // 2
+            cols = pl.ds(pl.multiple_of(n * SUB, SUB), SUB)
+            to = pl.ds(pl.multiple_of((n % 2) * SUB, SUB), SUB)
+            rows = hid[pl.ds(base, 2)].reshape(2 * TOK, 1152)
+            part = jnp.dot(rows[:, :1024], wd[:, :, cols].reshape(1024, SUB), preferred_element_type=f32)
+            part = part + jnp.dot(rows[:, 1024:], wdx[:, cols], preferred_element_type=f32)
+            xs[h, pl.ds(base, 2), :, to] = part.astype(jnp.bfloat16).reshape(2, TOK, SUB)
+            return carry
+
+        lax.fori_loop(0, 4, step, 0)
+
     for h, k in both:
         m1[h, k].wait_recv()
         f1[h, k].start()
@@ -171,21 +242,6 @@
         for d in (3, 1):
             for k in range(2):
                 m2[h, d, k].start()
-    for h, k in both:
-        m2[h, 0, k].wait_recv()
-        f2[h, 0, k].start()
-
-    pltpu.make_async_copy(wrow.at[pl.ds(0, 15)], wrow.at[pl.ds(0, 15)], x_recv.at[0]).wait()
-    columns = jnp.transpose(wrow[...].reshape(128, 256))
-    low_lane = lax.broadcasted_iota(jnp.int32, (TOK, 128), 1) < 64
-    for i in range(16):
-        wpat[i] = jnp.where(low_lane, columns[:TOK, 8 * i:8 * i + 1], columns[:TOK, 8 * i + 1:8 * i + 2])
-
-    for h, k in both:
-        f1[h, k].wait_recv()
-    for h in range(2):
-        for k in range(2):
-            m2[h, 2, k].start()
 
     def weights_on(i):
         w_p[i].wait_recv()
@@ -195,19 +251,46 @@
         w_fm[i].start()
         w_d[i, 1].start()
 
+    def weights_far(i):
+        w_fp[i].wait_recv()
+        w_fm[i].wait_recv()
+        w_d[i, 2].start()
+
     weights_on(0)
+
+    pltpu.make_async_copy(wrow.at[pl.ds(0, 15)], wrow.at[pl.ds(0, 15)], x_recv.at[0]).wait()
+    columns = jnp.transpose(wrow[...].reshape(128, 256))
+    low_lane = lax.broadcasted_iota(jnp.int32, (TOK, 128), 1) < 64
+    for i in range(16):
+        wpat[i] = jnp.where(low_lane, columns[:TOK, 8 * i:8 * i + 1], columns[:TOK, 8 * i + 1:8 * i + 2])
+
+    for h, k in both:
+        m2[h, 0, k].wait_recv()
+        f2[h, 0, k].start()
+    for i in range(2):
+        w_l[i].wait()
+        w_d[i, 0].wait_recv()
+    hidden(GROUPS[0], 0, 1)
+    for h, k in both:
+        f1[h, k].wait_recv()
+    for h in range(2):
+        for k in range(2):
+            m2[h, 2, k].start()
     own_side.wait()
     pltpu.make_async_copy(
         sb.at[0, :, pl.ds(0, 1920)], sb.at[0, :, pl.ds(0, 1920)], x_recv.at[1]).wait()
     sb_cross = remote(sb.at[0], sb.at[1], sb_dsend, sb_drecv, partner)
     sb_cross.start()
+    weights_on(1)
+    w_p[2].start()
+    w_m[2].start()
     for h, k in both:
         m2[h, 3, k].wait_recv()
         f2[h, 3, k].start()
-    weights_on(1)
-    for h, k in both:
-        m2[h, 1, k].wait_recv()
-        f2[h, 1, k].start()
+    for i in range(2):
+        w_d[i, 1].wait_recv()
+        w_d[i, 3].wait_recv()
+    hidden(GROUPS[0], 1, 2)
 
     @pl.when(jnp.logical_and(on_core, jnp.logical_not(is_src)))
     def _():
@@ -217,15 +300,6 @@
     @pl.when(jnp.logical_not(on_core))
     def _():
         sh_cross.wait_recv()
-
-    weights_on(2)
-    for h, k in both:
-        m2[h, 2, k].wait_recv()
-        f2[h, 2, k].start()
-    for i in range(3):
-        w_fp[i].wait_recv()
-        w_fm[i].wait_recv()
-        w_d[i, 2].start()
 
     sb_cross.wait_recv()
     wx[pl.ds(0, 64), :] = sb[core]
@@ -233,85 +307,79 @@
     wx[pl.ds(64, 32), :] = sh[0]
     wx[pl.ds(192, 32), :] = sh[1]
     wdx[pl.ds(64, 32), :] = sh[2]
-
-    for d in (0, 3, 1, 2):
+    dense_hidden(GROUPS[0])
+    for h, k in both:
+        m2[h, 1, k].wait_recv()
+        f2[h, 1, k].start()
+    weights_far(0)
+    hidden(GROUPS[1], 0, 3)
+    weights_far(1)
+    for h, k in both:
+        f2[h, 0, k].wait_recv()
+    for i in range(2):
+        w_d[i, 2].wait_recv()
+    hidden(GROUPS[0], 3, 1)
+    hidden(GROUPS[1], 3, 1)
+    for h, k in both:
+        m2[h, 2, k].wait_recv()
+        f2[h, 2, k].start()
+    for h, k in both:
+        f2[h, 3, k].wait_recv()
+    hidden(GROUPS[2], 0, 2)
+    weights_on(2)
+    hidden(GROUPS[2], 2, 2)
+    dense_hidden(GROUPS[1])
+    dense_hidden(GROUPS[2])
+    for d in (1, 2):
         for h, k in both:
             f2[h, d, k].wait_recv()
-    for i in range(3):
-        w_l[i].wait()
-        for dy in DY:
-            w_d[i, dy].wait_recv()
     for h in range(2):
         pltpu.make_async_copy(xs.at[h, pl.ds(0, 15)], xs.at[h, pl.ds(0, 15)], ag_send.at[h]).wait()
 
-    f32 = jnp.float32
-
-    def silu(v):
-        return v / (1.0 + jnp.exp(-v))
-
-    def both_halves(xa, xb, w):
-        return lax.dot_general(xa, w[:, :HALF], NT, preferred_element_type=f32) + lax.dot_general(
-            xb, w[:, HALF:], NT, preferred_element_type=f32)
-
-    def compute(group):
-        base = GROUP * group
-        pattern = wpat[pl.ds(base, GROUP)].reshape(ROWS, 128)
-
-        def up_step(c, carry):
-            xa = xs[0, pl.ds(base, GROUP)].reshape(ROWS, HALF)
-            xb = xs[1, pl.ds(base, GROUP)].reshape(ROWS, HALF)
-            rows = pl.ds(2 * c, 2)
-            gate = both_halves(xa, xb, wg[rows].reshape(256, D))
-            up = both_halves(xa, xb, wu[rows].reshape(256, D))
-            w2 = jnp.concatenate([pattern, pattern], axis=1)
-            hid[:, pl.ds(pl.multiple_of(c * 256, 256), 256)] = (silu(gate) * up * w2).astype(jnp.bfloat16)
-            return carry
-
-        lax.fori_loop(0, 4, up_step, 0)
-        xa = xs[0, pl.ds(base, GROUP)].reshape(ROWS, HALF)
-        xb = xs[1, pl.ds(base, GROUP)].reshape(ROWS, HALF)
-        dense = both_halves(xa, xb, wx[...])
-        first, second = dense[:, :128], dense[:, 128:]
-        lane = lax.broadcasted_iota(jnp.int32, (ROWS, 128), 1)
-        opening = 1.0 / (1.0 + jnp.exp(-second[:, :1]))
-        factor = jnp.where(lane < 64, opening, second)
-        hid[:, pl.ds(1024, 128)] = (silu(first) * factor).astype(jnp.bfloat16)
-
-        def down_step(n, carry):
-            h = n // 2
-            cols = pl.ds(pl.multiple_of(n * SUB, SUB), SUB)
-            to = pl.ds(pl.multiple_of((n % 2) * SUB, SUB), SUB)
-            part = jnp.dot(hid[:, :1024], wd[:, :, cols].reshape(1024, SUB), preferred_element_type=f32)
-            part = part + jnp.dot(hid[:, 1024:], wdx[:, cols], preferred_element_type=f32)
-            xs[h, pl.ds(base, GROUP), :, to] = part.astype(jnp.bfloat16).reshape(GROUP, TOK, SUB)
-            return carry
-
-        lax.fori_loop(0, 4, down_step, 0)
+    def last_hidden(part):
+        if part == "gu3a":
+            hidden(GROUPS[3], 0, 1)
+            weights_far(2)
+            hidden(GROUPS[3], 1, 1)
+            w_l[2].wait()
+            for dy in DY:
+                w_d[2, dy].wait_recv()
+        else:
+            hidden(GROUPS[3], 2, 2)
+            dense_hidden(GROUPS[3])
 
     rs_axes = [("z", "x"), ("x", "z")]
 
     def dst_slot(h, d1, q):
         return SLOT[(d1, q) if h == 0 else (q, d1)]
 
-    r1, s1, r2, s2 = {}, {}, {}, {}
+    r1, s1, e1, r2, s2, e2 = {}, {}, {}, {}, {}, {}
+    halves = [lo, hi]
     for h in range(2):
         b1, b2 = rs_axes[h]
         t = functools.partial(dst_slot, h)
-        for q in range(4):
-            r1[h, q, 0] = remote(
-                xs.at[h, t(2, q), :, lo], rl.at[h, q, 0], rs_send.at[h], rl_sem.at[h, q, 0], along(b1, 1))
-            r1[h, q, 1] = remote(
-                xs.at[h, t(2, q), :, hi], rl.at[h, q, 1], rs_send.at[h], rl_sem.at[h, q, 1], along(b1, 3))
-            s1[h, q, 0] = remote(
-                xs.at[h, t(1, q)], rf.at[h, q, 0], rs_send.at[h], rf_sem.at[h, q, 0], along(b1, 1))
-            s1[h, q, 1] = remote(
-                xs.at[h, t(3, q)], rf.at[h, q, 1], rs_send.at[h], rf_sem.at[h, q, 1], along(b1, 3))
-        r2[h, 0] = remote(
-            xs.at[h, t(0, 2), :, lo], rl2.at[h, 0], rs_send.at[h], rl2_sem.at[h, 0], along(b2, 1))
-        r2[h, 1] = remote(
-            xs.at[h, t(0, 2), :, hi], rl2.at[h, 1], rs_send.at[h], rl2_sem.at[h, 1], along(b2, 3))
-        s2[h, 0] = remote(xs.at[h, t(0, 1)], rf2.at[h, 0], rs_send.at[h], rf2_sem.at[h, 0], along(b2, 1))
-        s2[h, 1] = remote(xs.at[h, t(0, 3)], rf2.at[h, 1], rs_send.at[h], rf2_sem.at[h, 1], along(b2, 3))
+        for k in range(2):
+            sum_cols, own_cols = halves[k], halves[1 - k]
+            near, step = (1, 3)[k], (1, 3)[k]
+            for q in range(4):
+                to = along(b1, step)
+                r1[h, q, k] = remote(
+                    xs.at[h, t(2, q), :, sum_cols], rl.at[h, q, k], rs_send.at[h], rl_sem.at[h, q, k], to)
+                s1[h, q, k] = remote(
+                    xs.at[h, t(near, q), :, sum_cols], rf.at[h, q, k, :, sum_cols],
+                    rs_send.at[h], rf_sem.at[h, q, k, 0], to)
+                e1[h, q, k] = remote(
+                    xs.at[h, t(near, q), :, own_cols], rf.at[h, q, k, :, own_cols],
+                    rs_send.at[h], rf_sem.at[h, q, k, 1], to)
+            to = along(b2, step)
+            r2[h, k] = remote(
+                xs.at[h, t(0, 2), :, sum_cols], rl2.at[h, k], rs_send.at[h], rl2_sem.at[h, k], to)
+            s2[h, k] = remote(
+                xs.at[h, t(0, near), :, sum_cols], rf2.at[h, k, :, sum_cols],
+                rs_send.at[h], rf2_sem.at[h, k, 0], to)
+            e2[h, k] = remote(
+                xs.at[h, t(0, near), :, own_cols], rf2.at[h, k, :, own_cols],
+                rs_send.at[h], rf2_sem.at[h, k, 1], to)
 
     def add(slot, h, cols, *more):
         total = xs[h, slot, :, cols].astype(f32)
@@ -319,72 +387,43 @@
             total = total + m.astype(f32)
         xs[h, slot, :, cols] = total.astype(jnp.bfloat16)
 
-    halves = [lo, hi]
-    whole = pl.ds(0, HALF)
-
-    def relay(h, q):
-        for k in range(2):
+    for op in SUM_ORDER:
+        name = op[0]
+        if name == "C":
+            if op[1] in PAIRS:
+                down(PAIRS[op[1]])
+            else:
+                last_hidden(op[1])
+            continue
+        _, h, q, k = op
+        near = (1, 3)[k]
+        if name == "relay":
             r1[h, q, k].start()
-
-    def pass_on(h, q, k):
-        r1[h, q, k].wait_recv()
-        add(dst_slot(h, (1, 3)[k], q), h, halves[k], rl[h, q, k])
-        s1[h, q, k].start()
-
-    def collect(h, q):
-        for k in range(2):
-            s1[h, q, k].wait_recv()
-        add(dst_slot(h, 0, q), h, whole, rf[h, q, 0], rf[h, q, 1])
-
-    def relay2(h):
-        for k in range(2):
+        elif name == "free":
+            e1[h, q, k].start()
+        elif name == "pass":
+            r1[h, q, k].wait_recv()
+            add(dst_slot(h, near, q), h, halves[k], rl[h, q, k])
+            s1[h, q, k].start()
+        elif name == "collect":
+            for i in range(2):
+                e1[h, q, i].wait_recv()
+                s1[h, q, i].wait_recv()
+            add(dst_slot(h, 0, q), h, pl.ds(0, HALF), rf[h, q, 0], rf[h, q, 1])
+        elif name == "relay2":
             r2[h, k].start()
-
-    def pass_on2(h, k):
-        r2[h, k].wait_recv()
-        add(dst_slot(h, 0, (1, 3)[k]), h, halves[k], rl2[h, k])
-        s2[h, k].start()
-
-    compute(0)
-    relay(1, 2)
-    for q in (2, 1, 3, 0):
-        relay(0, q)
-    compute(1)
-    for q in (2, 1):
-        pass_on(0, q, 0)
-        pass_on(0, q, 1)
-    for k in range(2):
-        pass_on(1, 2, k)
-    relay(1, 1)
-    relay(1, 3)
-    compute(2)
-    for q in (3, 0):
-        pass_on(0, q, 0)
-        pass_on(0, q, 1)
-    for q in (1, 3):
-        for k in range(2):
-            pass_on(1, q, k)
-    collect(1, 2)
-    relay2(1)
-    compute(3)
-    relay(1, 0)
-    for q, k in ((1, 0), (3, 1)):
-        collect(1, q)
-        pass_on2(1, k)
-    for k in range(2):
-        pass_on(1, 0, k)
-    collect(0, 2)
-    relay2(0)
-    for q, k in ((1, 0), (3, 1)):
-        collect(0, q)
-        pass_on2(0, k)
-    collect(1, 0)
-    collect(0, 0)
-    for h in (1, 0):
-        for k in range(2):
-            s2[h, k].wait_recv()
-        total = xs[h, SLOT[0, 0]].astype(f32) + rf2[h, 0].astype(f32) + rf2[h, 1].astype(f32)
-        out_ref[:, pl.ds(h * HALF, HALF)] = total.astype(jnp.bfloat16)
+        elif name == "free2":
+            e2[h, k].start()
+        elif name == "pass2":
+            r2[h, k].wait_recv()
+            add(dst_slot(h, 0, near), h, halves[k], rl2[h, k])
+            s2[h, k].start()
+        else:
+            for i in range(2):
+                e2[h, i].wait_recv()
+                s2[h, i].wait_recv()
+            total = xs[h, SLOT[0, 0]].astype(f32) + rf2[h, 0].astype(f32) + rf2[h, 1].astype(f32)
+            out_ref[:, pl.ds(h * HALF, HALF)] = total.astype(jnp.bfloat16)
 
     for h in range(2):
         pltpu.make_async_copy(xs.at[h, pl.ds(0, 15)], xs.at[h, pl.ds(0, 15)], rs_send.at[h]).wait()
@@ -444,7 +483,7 @@
             vmem((128, D), bf16),
             vmem((2, 64, D), bf16),
             vmem((3, 32, D), bf16),
-            vmem((ROWS, 1152), bf16),
+            vmem((16, TOK, 1152), bf16),
             vmem((2, 4, 2, TOK, SUB), bf16),
             vmem((2, 4, 2, TOK, HALF), bf16),
             vmem((2, 2, TOK, SUB), bf16),
@@ -454,7 +493,7 @@
             dma((2,)), dma((2, 2)), dma((2, 2)), dma((2, 4, 2)), dma((2, 4, 2)),
             dma((3, 2)), dma((3, 2)), dma((3, 2)), dma((3, 2)), dma((3, 4)), dma((3, 4)), dma((3,)),
             dma((2,)), dma((2,)), dma((1,)), dma(()), dma(()), dma((3,)), dma(()), dma(()), dma(()), dma(()),
-            dma((2,)), dma((2, 4, 2)), dma((2, 4, 2)), dma((2, 2)), dma((2, 2)),
+            dma((2,)), dma((2, 4, 2)), dma((2, 4, 2, 2)), dma((2, 2)), dma((2, 2, 2)),
         ],
         compiler_params=pltpu.CompilerParams(
             collective_id=0, has_side_effects=True, vmem_limit_bytes=60 * 1024 * 1024),

time: 152 us -> 137 us (0.901)
  Pallas kernels: 145 us -> 131 us
    pallas_call x1, Pallas kernels: 145 us -> 131 us  [body(): pl.pallas_call(kernel, out_shape=jax.ShapeDtypeStruct((TOK, D), bf16), in...]
where the time goes in v2:
time: 137 us
  Pallas kernels  131 us (96%)
  local copies, waits for them, and re-layouts  5.08 us (4%)
    pallas_call x1, Pallas kernels, body(): pl.pallas_call(kernel, out_shape=jax.ShapeDtypeStruct((TOK, D), bf16), in...  131 us
    unnamed x17, local copies, waits for them, and re-layouts  2.88 us

profile of v2, /device:TPU:1, one launch (start us, length us, event | category | flops | bytes accessed | tf_op | source)
XLA Modules:
  0.0 136.8 jit_solution(5812898506152422102)
XLA Ops:
  0.0 0.0 copy-start
  0.0 0.0 copy-start.7
  0.0 0.0 copy-start.6
  0.0 0.0 copy-start.5
  0.0 0.7 copy-done.7
  0.7 0.0 copy-done.6
  0.8 0.0 copy-done.5
  0.8 0.1 select_reduce_fusion
  0.9 0.0 copy-start.2
  0.9 0.0 copy-start.1
  0.9 0.6 pad.9.sgate_ref
  1.5 0.7 pad.8.w8_ref
  2.2 0.0 copy-done
  2.2 0.0 copy-done.2
  2.2 0.0 copy-done.1
  2.3 0.0 copy-start.3
  2.3 0.0 copy-start.4
  2.3 0.8 copy.15
  3.2 0.1 copy-done.3
  3.2 0.1 copy-done.4
  3.4 0.8 pad_maximum_fusion.shared_hbm
  4.1 130.7 %routed_layer.1 = bf16[144,2048]{1,0:T(8,128)(2,1)} custom-call(bf16[144,2048]{1,0:T(8,128)(2,1)} %tok_ref.1, f32[1,2048]{1,0:T(1,128)} %bitcast.19, f32[16,8,256]{2,1,0:T(8,128)} %pad.8.w8_ref, bf16[128,2048]{1,0:T(8,128)(2,1)} %bitcast.16, bf16[128,2048]{1,0:T(8,128)(2,1)} %bitcast.17, bf16[128,2048]{1,0:T(8,128)(2,1)} %bitcast.18, ...), custom_call_target="tpu_custom_call" | custom-call | tf_op jit(solution)/shard_map/routed_layer/pallas_call | solution.py:472
  134.9 1.9 %copy.17 = bf16[144,2048]{1,0:T(8,128)(2,1)} copy(bf16[144,2048]{1,0:T(8,128)(2,1)} %routed_layer.1) | data formatting | bytes 1179648
  (5 shorter events, 0.1 us)
Async XLA Ops:
  0.0 2.2 %copy-start = (bf16[64,2048]{1,0:T(8,128)(2,1)S(1)}, bf16[64,2048]{1,0:T(8,128)(2,1)}, u32[]{:S(2)}) copy-start(bf16[64,2048]{1,0:T(8,128)(2,1)} %param.20) | copy-start | bytes 786436
  0.0 0.7 copy-start.7
  0.0 0.8 copy-start.6
  0.0 0.8 copy-start.5
  0.9 1.4 %copy-start.2 = (bf16[128,1024]{1,0:T(8,128)(2,1)S(1)}, bf16[128,1024]{1,0:T(8,128)(2,1)}, u32[]{:S(2)}) copy-start(bf16[128,1024]{1,0:T(8,128)(2,1)} %param.24) | copy-start | bytes 786436
  0.9 1.3 copy-start.1
  2.3 1.0 copy-start.3
  2.3 1.0 copy-start.4

commit v3 on v2

--- a/solution.py
+++ b/solution.py
@@ -22,25 +22,23 @@
     (1, 0), (0, 1), (0, 3), (0, 0),
 ]
 GROUPS = [12, 8, 4, 0]
-PAIRS = {
-    "g3a": 0, "g3b": 2, "g2a": 4, "g2b": 6, "g1a": 8, "g1b": 10, "g0a": 12, "g0b": 14,
-}
+PARTS = {"g3a": (0, 2), "g3b": (2, 2), "g2a": (4, 2), "g2b": (6, 2), "g1": (8, 4), "g0": (12, 4)}
 SUM_ORDER = [
-    ("C", "gu3a"), ("C", "g2b"), ("relay", 1, 0, 1), ("relay", 1, 0, 0), ("relay", 0, 0, 0), ("relay", 0, 0, 1),
-    ("C", "g1a"), ("free", 0, 3, 0), ("free", 1, 1, 0), ("free", 0, 1, 0), ("free", 1, 1, 1), ("C", "g2a"),
-    ("relay", 1, 3, 0), ("relay", 1, 3, 1), ("free", 0, 2, 1), ("free", 0, 3, 1), ("free", 1, 3, 1), ("C", "gu3b"),
-    ("C", "g3a"), ("relay", 1, 2, 0), ("relay", 0, 2, 1), ("relay", 0, 2, 0), ("relay", 1, 2, 1), ("relay", 1, 1, 1),
-    ("free", 0, 2, 0), ("relay", 1, 1, 0), ("C", "g3b"), ("relay", 0, 3, 1), ("relay", 0, 3, 0), ("free", 1, 2, 1),
-    ("free", 1, 2, 0), ("relay", 0, 1, 1), ("relay", 0, 1, 0), ("C", "g0a"), ("pass", 1, 3, 1), ("free", 1, 0, 0),
-    ("pass", 0, 0, 0), ("pass", 1, 0, 0), ("free", 0, 0, 0), ("C", "g1b"), ("free", 1, 3, 0), ("pass", 1, 2, 0),
-    ("pass", 0, 2, 1), ("pass", 0, 2, 0), ("pass", 1, 3, 0), ("free", 0, 1, 1), ("free", 0, 0, 1), ("pass", 0, 0, 1),
-    ("C", "g0b"), ("pass", 1, 2, 1), ("pass", 0, 3, 1), ("free", 1, 0, 1), ("pass", 1, 1, 0), ("pass", 1, 0, 1),
-    ("pass", 0, 3, 0), ("pass", 1, 1, 1), ("pass", 0, 1, 1), ("pass", 0, 1, 0), ("collect", 0, 2, 0),
+    ("C", "g2b"), ("relay", 1, 0, 0), ("relay", 0, 0, 1), ("relay", 1, 0, 1), ("relay", 0, 0, 0), ("C", "g1"),
+    ("free", 0, 3, 0), ("free", 1, 3, 0), ("free", 0, 0, 1), ("free", 0, 1, 0), ("free", 0, 1, 1), ("free", 1, 1, 0),
+    ("free", 1, 1, 1), ("C", "g0"), ("free", 0, 0, 0), ("free", 1, 0, 0), ("free", 1, 0, 1), ("pass", 0, 0, 1),
+    ("pass", 1, 0, 1), ("pass", 1, 0, 0), ("pass", 0, 0, 0), ("C", "g2a"), ("free", 0, 2, 1), ("relay", 1, 3, 0),
+    ("relay", 1, 3, 1), ("free", 1, 3, 1), ("free", 0, 3, 1), ("C", "x"), ("C", "y"), ("C", "g3a"),
+    ("relay", 0, 2, 0), ("relay", 0, 2, 1), ("relay", 1, 2, 0), ("relay", 1, 2, 1), ("free", 0, 2, 0),
+    ("relay", 1, 1, 1), ("relay", 1, 1, 0), ("C", "g3b"), ("relay", 0, 3, 0), ("relay", 0, 3, 1), ("free", 1, 2, 0),
+    ("free", 1, 2, 1), ("collect", 0, 0, 0), ("relay", 0, 1, 1), ("relay", 0, 1, 0), ("collect", 1, 0, 0),
+    ("S", "near"), ("pass", 1, 3, 1), ("pass", 1, 3, 0), ("pass", 0, 2, 0), ("pass", 1, 2, 0), ("pass", 0, 2, 1),
+    ("pass", 1, 2, 1), ("pass", 0, 3, 1), ("pass", 1, 1, 0), ("pass", 1, 1, 1), ("pass", 0, 3, 0), ("pass", 0, 1, 1),
+    ("S", "far"), ("pass", 0, 1, 0), ("collect", 1, 3, 0), ("free2", 1, 0, 1), ("S", "work"), ("collect", 0, 2, 0),
     ("relay2", 0, 0, 0), ("relay2", 0, 0, 1), ("collect", 1, 2, 0), ("relay2", 1, 0, 0), ("relay2", 1, 0, 1),
-    ("collect", 0, 0, 0), ("collect", 1, 3, 0), ("free2", 1, 0, 1), ("collect", 0, 3, 0), ("free2", 0, 0, 1),
-    ("collect", 1, 0, 0), ("collect", 1, 1, 0), ("free2", 1, 0, 0), ("collect", 0, 1, 0), ("free2", 0, 0, 0),
-    ("pass2", 0, 0, 0), ("pass2", 0, 0, 1), ("pass2", 1, 0, 0), ("pass2", 1, 0, 1), ("final", 0, 0, 0),
-    ("final", 1, 0, 0),
+    ("collect", 0, 3, 0), ("free2", 0, 0, 1), ("collect", 1, 1, 0), ("free2", 1, 0, 0), ("collect", 0, 1, 0),
+    ("free2", 0, 0, 0), ("pass2", 0, 0, 0), ("pass2", 0, 0, 1), ("pass2", 1, 0, 0), ("pass2", 1, 0, 1),
+    ("final", 0, 0, 0), ("final", 1, 0, 0),
 ]
 SLOT = {place: i for i, place in enumerate(ORDER)}
 DY = [0, 1, 3, 2]
@@ -49,12 +47,15 @@
 
 
 def kernel(
-    tok_ref, gain_ref, w8_ref, gate_hbm, up_hbm, down_hbm, shared_hbm, side_hbm, sgate_ref,
+    tok_hbm, gain_hbm, ids_hbm, route_hbm, gate_hbm, up_hbm, down_hbm, sg_hbm, su_hbm, sd_hbm,
+    side_in_hbm, side_out_hbm, sgate_hbm,
     out_ref,
-    xs, wg, wu, wd, wx, wdx, sb, sh, hid, rl, rf, rl2, rf2, wrow, wpat,
+    tok_ref, gain_ref, ids_ref, route_ref, side_ref, sgate_ref, in_sem,
+    xs, own, wg, wu, wd, wx, wdx, sb, sp, sg, su, sd, shid, sout, hid, rl, rf, rl2, rf2, w8, wrow, wpat,
     ag_send, ag_m1, ag_f1, ag_m2, ag_f2,
-    w_send, w_recv, w_fsend, w_frecv, w_dsend, w_drecv, w_loc,
-    x_send, x_recv, x_loc, sb_dsend, sb_drecv, sh_send, sh_recv, sh_dsend, sh_drecv, sh_loc,
+    w_send, w_recv, w_fsend, w_frecv, w_dsend, w_drecv, w_loc, late_send, late_recv,
+    x_send, x_recv, sb_dsend, sb_drecv,
+    s_send, s_recv, s_fsend, s_frecv, s_dsend, s_drecv, s_loc,
     rs_send, rl_sem, rf_sem, rl2_sem, rf2_sem,
 ):
     ep = lax.axis_index("ep")
@@ -79,23 +80,69 @@
             device_id_type=pl.DeviceIdType.MESH,
         )
 
-    wx[pl.ds(96, 32), :] = jnp.zeros((32, D), jnp.bfloat16)
-    wx[pl.ds(128, 16), :] = sgate_ref[...]
-    wx[pl.ds(144, 48), :] = jnp.zeros((48, D), jnp.bfloat16)
-    wx[pl.ds(224, 32), :] = jnp.zeros((32, D), jnp.bfloat16)
-    wdx[pl.ds(96, 32), :] = jnp.zeros((32, D), jnp.bfloat16)
+    loads = [
+        pltpu.make_async_copy(src, dst, in_sem.at[i])
+        for i, (src, dst) in enumerate([
+            (tok_hbm, tok_ref), (gain_hbm, gain_ref), (ids_hbm, ids_ref), (route_hbm, route_ref),
+            (sgate_hbm, sgate_ref)])
+    ]
+    for c in loads:
+        c.start()
+    side_load = pltpu.make_async_copy(side_in_hbm, side_ref, in_sem.at[5])
+    other_load = pltpu.make_async_copy(side_out_hbm, side_ref, in_sem.at[5])
+
+    @pl.when(core == 0)
+    def _():
+        side_load.start()
+
+    @pl.when(core == 1)
+    def _():
+        other_load.start()
 
     barrier = pltpu.get_barrier_semaphore()
     peers = [at_ep(*p) for p in ORDER if p != (0, 0)] + [at_y(d) for d in (1, 2, 3)] + [partner]
     for peer in peers:
         pl.semaphore_signal(barrier, inc=1, device_id=peer, device_id_type=pl.DeviceIdType.MESH)
+
+    f32 = jnp.float32
+    for c in loads:
+        c.wait()
+    values = tok_ref[...].astype(f32)
+    scale_inv = lax.rsqrt(jnp.mean(values * values, axis=-1, keepdims=True) + norm_eps)
+    normed = (values * scale_inv * gain_ref[...]).astype(jnp.bfloat16)
+    own[0] = normed[:, :HALF]
+    own[1] = normed[:, HALF:]
+    xs[0, SLOT[0, 0]] = normed[:, :HALF]
+    xs[1, SLOT[0, 0]] = normed[:, HALF:]
+    expert = lax.broadcasted_iota(jnp.int32, (32, TOK), 0)
+    dense_weight = jnp.zeros((32, TOK), f32)
+    for k in range(8):
+        dense_weight += jnp.where(ids_ref[k:k + 1, :] == expert, route_ref[k:k + 1, :], 0.0)
+    w8[...] = jnp.zeros((16, 8, 128), f32)
+    for e in range(32):
+        w8[e // 2, pl.ds(2 * (e % 2), 1), :] = dense_weight[e:e + 1, :128]
+        w8[e // 2, pl.ds(2 * (e % 2) + 1, 1), pl.ds(0, TOK - 128)] = dense_weight[e:e + 1, 128:]
+
+    side_load.wait()
+    for j in range(8):
+        block = jnp.transpose(side_ref[:, pl.ds(128 * j, 128)].astype(f32)).astype(jnp.bfloat16)
+        sp[2 * j] = block[:64]
+        sp[2 * j + 1] = block[64:]
+    top_row = lax.broadcasted_iota(jnp.int32, (16, 128), 0) == 0
+    for j in range(16):
+        part = sgate_ref[j:j + 1, :].astype(f32)
+        wx[pl.ds(64, 16), pl.ds(128 * j, 128)] = jnp.where(top_row, part, 0.0).astype(jnp.bfloat16)
+    wx[pl.ds(80, 48), :] = jnp.zeros((48, D), jnp.bfloat16)
+    wdx[pl.ds(64, 64), :] = jnp.zeros((64, D), jnp.bfloat16)
+
     pl.semaphore_wait(barrier, len(peers))
 
     big = [(gate_hbm, wg), (up_hbm, wu), (down_hbm, wd)]
     w_p, w_m, w_fp, w_fm, w_d, w_l = [], [], [], [], {}, []
     for i, (src, dst) in enumerate(big):
-        w_p.append(remote(src, dst.at[2 * DYI[3]], w_send.at[i, 0], w_recv.at[i, 0], at_y(1)))
-        w_m.append(remote(src, dst.at[2 * DYI[1]], w_send.at[i, 1], w_recv.at[i, 1], at_y(3)))
+        if i < 2:
+            w_p.append(remote(src, dst.at[2 * DYI[3]], w_send.at[i, 0], w_recv.at[i, 0], at_y(1)))
+            w_m.append(remote(src, dst.at[2 * DYI[1]], w_send.at[i, 1], w_recv.at[i, 1], at_y(3)))
         w_fp.append(remote(
             dst.at[2 * DYI[3], pl.ds(0, 64)], dst.at[2 * DYI[2], pl.ds(0, 64)],
             w_fsend.at[i, 0], w_frecv.at[i, 0], at_y(1)))
@@ -107,18 +154,19 @@
                 src if dy == 0 else dst.at[2 * DYI[dy]], dst.at[2 * DYI[dy] + 1],
                 w_dsend.at[i, dy], w_drecv.at[i, dy], partner)
         w_l.append(pltpu.make_async_copy(src, dst.at[0], w_loc.at[i]))
+    first_rows, last_rows = pl.ds(0, 64), pl.ds(64, 64)
+    late_p = [
+        remote(down_hbm.at[r], wd.at[2 * DYI[3], r], late_send.at[i, 0], late_recv.at[i, 0], at_y(1))
+        for i, r in enumerate((first_rows, last_rows))]
+    late_m = [
+        remote(down_hbm.at[r], wd.at[2 * DYI[1], r], late_send.at[i, 1], late_recv.at[i, 1], at_y(3))
+        for i, r in enumerate((last_rows, first_rows))]
     for i in range(2):
         w_p[i].start()
         w_m[i].start()
     for i in range(3):
         w_d[i, 0].start()
         w_l[i].start()
-
-    values = tok_ref[...].astype(jnp.float32)
-    scale_inv = lax.rsqrt(jnp.mean(values * values, axis=-1, keepdims=True) + norm_eps)
-    normed = (values * scale_inv * gain_ref[...]).astype(jnp.bfloat16)
-    xs[0, SLOT[0, 0]] = normed[:, :HALF]
-    xs[1, SLOT[0, 0]] = normed[:, HALF:]
 
     axes = [("x", "z"), ("z", "x")]
 
@@ -156,36 +204,34 @@
     for dz, dx in ORDER[:-1]:
         there = at_ep(dz, dx)
         mine = SLOT[(4 - dz) % 4, (4 - dx) % 4]
-        w_small.append(remote(w8_ref.at[there[0]], wrow.at[mine], x_send.at[0], x_recv.at[0], there))
+        w_small.append(remote(
+            w8.at[there[0]], wrow.at[mine], x_send.at[0], x_recv.at[0], there))
         s_small.append(remote(
-            side_hbm.at[there[0]], sb.at[0, :, pl.ds(pl.multiple_of(ep * 128, 128), 128)],
+            sp.at[there[0]], sb.at[0, :, pl.ds(pl.multiple_of(ep * 128, 128), 128)],
             x_send.at[1], x_recv.at[1], there))
     for c in w_small + s_small:
         c.start()
-    own_side = pltpu.make_async_copy(
-        side_hbm.at[ep], sb.at[0, :, pl.ds(pl.multiple_of(ep * 128, 128), 128)], x_loc.at[0])
-    own_side.start()
-    wrow[SLOT[0, 0]] = w8_ref[ep]
+    sb[0, :, pl.ds(pl.multiple_of(ep * 128, 128), 128)] = sp[ep]
+    wrow[SLOT[0, 0]] = w8[ep]
 
     for h, k in both:
         m2[h, 0, k].start()
 
-    owner = ep // 2
-    is_src = tp == owner
-    on_core = core == owner % 2
-    sh_copies = [remote(shared_hbm, sh, sh_send.at[d - 1], sh_recv, at_y(d)) for d in (1, 2, 3)]
-    sh_cross = remote(sh, sh, sh_dsend, sh_drecv, partner)
-    sh_own = pltpu.make_async_copy(shared_hbm, sh, sh_loc)
-
-    @pl.when(is_src)
-    def _():
-        for c in sh_copies:
-            c.start()
-        sh_own.start()
-        sh_own.wait()
-        sh_cross.start()
-
-    f32 = jnp.float32
+    s_p, s_m, s_fp, s_fm, s_d, s_l = [], [], [], [], {}, []
+    for i, (src, dst) in enumerate([(sg_hbm, sg), (su_hbm, su), (sd_hbm, sd)]):
+        s_p.append(remote(src, dst.at[2 * DYI[3]], s_send.at[i, 0], s_recv.at[i, 0], at_y(1)))
+        s_m.append(remote(src, dst.at[2 * DYI[1]], s_send.at[i, 1], s_recv.at[i, 1], at_y(3)))
+        s_fp.append(remote(
+            dst.at[2 * DYI[3], pl.ds(0, 32)], dst.at[2 * DYI[2], pl.ds(0, 32)],
+            s_fsend.at[i, 0], s_frecv.at[i, 0], at_y(1)))
+        s_fm.append(remote(
+            dst.at[2 * DYI[1], pl.ds(32, 32)], dst.at[2 * DYI[2], pl.ds(32, 32)],
+            s_fsend.at[i, 1], s_frecv.at[i, 1], at_y(3)))
+        for dy in DY:
+            s_d[i, dy] = remote(
+                src if dy == 0 else dst.at[2 * DYI[dy]], dst.at[2 * DYI[dy] + 1],
+                s_dsend.at[i, dy], s_drecv.at[i, dy], partner)
+        s_l.append(pltpu.make_async_copy(src, dst.at[0], s_loc.at[i]))
 
     def silu(v):
         return v / (1.0 + jnp.exp(-v))
@@ -215,22 +261,55 @@
     def dense_hidden(base):
         xa, xb = rows_of(base)
         dense = both_halves(xa, xb, wx[...])
-        first, second = dense[:, :128], dense[:, 128:]
         lane = lax.broadcasted_iota(jnp.int32, (ROWS, 128), 1)
-        opening = 1.0 / (1.0 + jnp.exp(-second[:, :1]))
-        factor = jnp.where(lane < 64, opening, second)
-        value = (silu(first) * factor).astype(jnp.bfloat16)
+        opening = 1.0 / (1.0 + jnp.exp(-dense[:, 64:65]))
+        value = jnp.where(lane < 64, silu(dense) * opening, 0.0).astype(jnp.bfloat16)
         hid[pl.ds(base, GROUP), :, pl.ds(1024, 128)] = value.reshape(GROUP, TOK, 128)
 
-    def down(base):
+    def shared_expert():
+        for c in range(2):
+            rows = pl.ds(4 * c, 4)
+            gate = both_halves(own[0], own[1], sg[rows].reshape(256, D))
+            up = both_halves(own[0], own[1], su[rows].reshape(256, D))
+            shid[:, pl.ds(256 * c, 256)] = (silu(gate) * up).astype(jnp.bfloat16)
+
+        def step(n, carry):
+            cols = pl.ds(pl.multiple_of(n * SUB, SUB), SUB)
+            sout[:, cols] = jnp.dot(shid[...], sd[:, :, cols].reshape(512, SUB), preferred_element_type=f32)
+            return carry
+
+        lax.fori_loop(0, 4, step, 0)
+
+    def shared_step(part):
+        if part == "near":
+            for i in range(3):
+                s_p[i].wait_recv()
+                s_fp[i].start()
+                s_d[i, 3].start()
+                s_m[i].wait_recv()
+                s_fm[i].start()
+                s_d[i, 1].start()
+        elif part == "far":
+            for i in range(3):
+                s_fp[i].wait_recv()
+                s_fm[i].wait_recv()
+                s_d[i, 2].start()
+        else:
+            for i in range(3):
+                s_l[i].wait()
+                for dy in DY:
+                    s_d[i, dy].wait_recv()
+            shared_expert()
+
+    def down(base, count):
         def step(n, carry):
             h = n // 2
             cols = pl.ds(pl.multiple_of(n * SUB, SUB), SUB)
             to = pl.ds(pl.multiple_of((n % 2) * SUB, SUB), SUB)
-            rows = hid[pl.ds(base, 2)].reshape(2 * TOK, 1152)
+            rows = hid[pl.ds(base, count)].reshape(count * TOK, 1152)
             part = jnp.dot(rows[:, :1024], wd[:, :, cols].reshape(1024, SUB), preferred_element_type=f32)
             part = part + jnp.dot(rows[:, 1024:], wdx[:, cols], preferred_element_type=f32)
-            xs[h, pl.ds(base, 2), :, to] = part.astype(jnp.bfloat16).reshape(2, TOK, SUB)
+            xs[h, pl.ds(base, count), :, to] = part.astype(jnp.bfloat16).reshape(count, TOK, SUB)
             return carry
 
         lax.fori_loop(0, 4, step, 0)
@@ -259,10 +338,13 @@
     weights_on(0)
 
     pltpu.make_async_copy(wrow.at[pl.ds(0, 15)], wrow.at[pl.ds(0, 15)], x_recv.at[0]).wait()
-    columns = jnp.transpose(wrow[...].reshape(128, 256))
-    low_lane = lax.broadcasted_iota(jnp.int32, (TOK, 128), 1) < 64
+    columns = jnp.transpose(wrow[...].reshape(128, 128))
+    low_lane = lax.broadcasted_iota(jnp.int32, (128, 128), 1) < 64
     for i in range(16):
-        wpat[i] = jnp.where(low_lane, columns[:TOK, 8 * i:8 * i + 1], columns[:TOK, 8 * i + 1:8 * i + 2])
+        first, last, c = columns, columns[:TOK - 128], 8 * i
+        wpat[i, pl.ds(0, 128)] = jnp.where(low_lane, first[:, c:c + 1], first[:, c + 2:c + 3])
+        wpat[i, pl.ds(128, TOK - 128)] = jnp.where(
+            low_lane[:TOK - 128], last[:, c + 1:c + 2], last[:, c + 3:c + 4])
 
     for h, k in both:
         m2[h, 0, k].wait_recv()
@@ -276,14 +358,14 @@
     for h in range(2):
         for k in range(2):
             m2[h, 2, k].start()
-    own_side.wait()
     pltpu.make_async_copy(
         sb.at[0, :, pl.ds(0, 1920)], sb.at[0, :, pl.ds(0, 1920)], x_recv.at[1]).wait()
     sb_cross = remote(sb.at[0], sb.at[1], sb_dsend, sb_drecv, partner)
     sb_cross.start()
     weights_on(1)
-    w_p[2].start()
-    w_m[2].start()
+    for i in range(2):
+        late_p[i].start()
+        late_m[i].start()
     for h, k in both:
         m2[h, 3, k].wait_recv()
         f2[h, 3, k].start()
@@ -292,21 +374,9 @@
         w_d[i, 3].wait_recv()
     hidden(GROUPS[0], 1, 2)
 
-    @pl.when(jnp.logical_and(on_core, jnp.logical_not(is_src)))
-    def _():
-        sh_copies[0].wait_recv()
-        sh_cross.start()
-
-    @pl.when(jnp.logical_not(on_core))
-    def _():
-        sh_cross.wait_recv()
-
     sb_cross.wait_recv()
     wx[pl.ds(0, 64), :] = sb[core]
     wdx[pl.ds(0, 64), :] = sb[1 - core]
-    wx[pl.ds(64, 32), :] = sh[0]
-    wx[pl.ds(192, 32), :] = sh[1]
-    wdx[pl.ds(64, 32), :] = sh[2]
     dense_hidden(GROUPS[0])
     for h, k in both:
         m2[h, 1, k].wait_recv()
@@ -320,15 +390,28 @@
         w_d[i, 2].wait_recv()
     hidden(GROUPS[0], 3, 1)
     hidden(GROUPS[1], 3, 1)
+    late_p[0].wait_recv()
+    w_fp[2].start()
+    late_m[0].wait_recv()
+    w_fm[2].start()
+    for i in range(3):
+        s_p[i].start()
+        s_m[i].start()
+    for i in range(3):
+        s_d[i, 0].start()
+        s_l[i].start()
     for h, k in both:
         m2[h, 2, k].wait_recv()
         f2[h, 2, k].start()
+    dense_hidden(GROUPS[1])
     for h, k in both:
         f2[h, 3, k].wait_recv()
-    hidden(GROUPS[2], 0, 2)
-    weights_on(2)
-    hidden(GROUPS[2], 2, 2)
-    dense_hidden(GROUPS[1])
+    late_p[1].wait_recv()
+    w_d[2, 3].start()
+    late_m[1].wait_recv()
+    w_d[2, 1].start()
+    hidden(GROUPS[2], 0, 4)
+    weights_far(2)
     dense_hidden(GROUPS[2])
     for d in (1, 2):
         for h, k in both:
@@ -336,14 +419,13 @@
     for h in range(2):
         pltpu.make_async_copy(xs.at[h, pl.ds(0, 15)], xs.at[h, pl.ds(0, 15)], ag_send.at[h]).wait()
 
+    w_l[2].wait()
+    for dy in DY:
+        w_d[2, dy].wait_recv()
+
     def last_hidden(part):
-        if part == "gu3a":
-            hidden(GROUPS[3], 0, 1)
-            weights_far(2)
-            hidden(GROUPS[3], 1, 1)
-            w_l[2].wait()
-            for dy in DY:
-                w_d[2, dy].wait_recv()
+        if part == "x":
+            hidden(GROUPS[3], 0, 2)
         else:
             hidden(GROUPS[3], 2, 2)
             dense_hidden(GROUPS[3])
@@ -390,10 +472,13 @@
     for op in SUM_ORDER:
         name = op[0]
         if name == "C":
-            if op[1] in PAIRS:
-                down(PAIRS[op[1]])
+            if op[1] in PARTS:
+                down(*PARTS[op[1]])
             else:
                 last_hidden(op[1])
+            continue
+        if name == "S":
+            shared_step(op[1])
             continue
         _, h, q, k = op
         near = (1, 3)[k]
@@ -423,85 +508,88 @@
                 e2[h, i].wait_recv()
                 s2[h, i].wait_recv()
             total = xs[h, SLOT[0, 0]].astype(f32) + rf2[h, 0].astype(f32) + rf2[h, 1].astype(f32)
+            total = total + sout[:, pl.ds(h * HALF, HALF)]
             out_ref[:, pl.ds(h * HALF, HALF)] = total.astype(jnp.bfloat16)
 
     for h in range(2):
         pltpu.make_async_copy(xs.at[h, pl.ds(0, 15)], xs.at[h, pl.ds(0, 15)], rs_send.at[h]).wait()
-    for i in range(3):
+    for i in range(2):
         w_p[i].wait_send()
         w_m[i].wait_send()
+        late_p[i].wait_send()
+        late_m[i].wait_send()
+    for i in range(3):
         w_fp[i].wait_send()
         w_fm[i].wait_send()
+        s_p[i].wait_send()
+        s_m[i].wait_send()
+        s_fp[i].wait_send()
+        s_fm[i].wait_send()
         for dy in DY:
             w_d[i, dy].wait_send()
+            s_d[i, dy].wait_send()
     pltpu.make_async_copy(wrow.at[pl.ds(0, 15)], wrow.at[pl.ds(0, 15)], x_send.at[0]).wait()
     pltpu.make_async_copy(
         sb.at[0, :, pl.ds(0, 1920)], sb.at[0, :, pl.ds(0, 1920)], x_send.at[1]).wait()
     sb_cross.wait_send()
 
-    @pl.when(is_src)
-    def _():
-        for c in sh_copies:
-            c.wait_send()
-
-    @pl.when(on_core)
-    def _():
-        sh_cross.wait_send()
-
 
 def body(
     tokens, norm_gain, expert_ids, route_weights, expert_gate, expert_up, expert_down,
     shared_gate, shared_up, shared_down, side_in, side_out, side_gate,
 ):
-    ep = lax.axis_index("ep")
-    core = lax.axis_index("tp") % 2
-    experts = jnp.arange(32, dtype=jnp.int32)
-    chosen = expert_ids.T[None, :, :] == experts[:, None, None]
-    dense = jnp.sum(jnp.where(chosen, route_weights.T[None, :, :], 0.0), axis=1)
-    w8 = jnp.pad(dense.reshape(16, 2, TOK), ((0, 0), (0, 6), (0, 256 - TOK)))
-    side = jnp.where(core == 0, side_in, side_out).T.reshape(16, 64, 128)
-    first = (ep % 2) * 32
-    shared = jnp.stack([
-        lax.dynamic_slice_in_dim(a, first, 32, axis=0) for a in (shared_gate, shared_up, shared_down)
-    ])
-    sgate = jnp.pad(side_gate.reshape(1, D), ((0, 15), (0, 0)))
     bf16, f32 = jnp.bfloat16, jnp.float32
     dma, vmem = pltpu.SemaphoreType.DMA, pltpu.VMEM
     in_vmem = pl.BlockSpec(memory_space=pltpu.VMEM)
     in_any = pl.BlockSpec(memory_space=pl.ANY)
     return pl.pallas_call(
         kernel,
-        out_shape=jax.ShapeDtypeStruct((TOK, D), bf16),
-        in_specs=[in_vmem, in_vmem, in_vmem] + [in_any] * 5 + [in_vmem],
+        out_shape=pltpu.VMEM((TOK, D), bf16),
+        in_specs=[in_any] * 13,
         out_specs=in_vmem,
         scratch_shapes=[
+            vmem((TOK, D), bf16),
+            vmem((1, D), f32),
+            vmem((8, TOK), jnp.int32),
+            vmem((8, TOK), f32),
+            vmem((128, 1024), bf16),
+            vmem((16, 128), bf16),
+            dma((6,)),
             vmem((2, 16, TOK, HALF), bf16),
+            vmem((2, TOK, HALF), bf16),
             vmem((8, 128, D), bf16),
             vmem((8, 128, D), bf16),
             vmem((8, 128, D), bf16),
-            vmem((256, D), bf16),
+            vmem((128, D), bf16),
             vmem((128, D), bf16),
             vmem((2, 64, D), bf16),
-            vmem((3, 32, D), bf16),
+            vmem((16, 64, 128), bf16),
+            vmem((8, 64, D), bf16),
+            vmem((8, 64, D), bf16),
+            vmem((8, 64, D), bf16),
+            vmem((TOK, 512), bf16),
+            vmem((TOK, D), f32),
             vmem((16, TOK, 1152), bf16),
             vmem((2, 4, 2, TOK, SUB), bf16),
             vmem((2, 4, 2, TOK, HALF), bf16),
             vmem((2, 2, TOK, SUB), bf16),
             vmem((2, 2, TOK, HALF), bf16),
-            vmem((16, 8, 256), f32),
+            vmem((16, 8, 128), f32),
+            vmem((16, 8, 128), f32),
             vmem((16, TOK, 128), f32),
             dma((2,)), dma((2, 2)), dma((2, 2)), dma((2, 4, 2)), dma((2, 4, 2)),
+            dma((2, 2)), dma((2, 2)), dma((3, 2)), dma((3, 2)), dma((3, 4)), dma((3, 4)), dma((3,)),
+            dma((2, 2)), dma((2, 2)), dma((2,)), dma((2,)), dma(()), dma(()),
             dma((3, 2)), dma((3, 2)), dma((3, 2)), dma((3, 2)), dma((3, 4)), dma((3, 4)), dma((3,)),
-            dma((2,)), dma((2,)), dma((1,)), dma(()), dma(()), dma((3,)), dma(()), dma(()), dma(()), dma(()),
             dma((2,)), dma((2, 4, 2)), dma((2, 4, 2, 2)), dma((2, 2)), dma((2, 2, 2)),
         ],
         compiler_params=pltpu.CompilerParams(
             collective_id=0, has_side_effects=True, vmem_limit_bytes=60 * 1024 * 1024),
         name="routed_layer",
     )(
-        tokens, norm_gain.reshape(1, D), w8,
+        tokens, norm_gain.reshape(1, D), expert_ids.T, route_weights.T,
         expert_gate.reshape(128, D), expert_up.reshape(128, D), expert_down.reshape(128, D),
-        shared, side, sgate,
+        shared_gate, shared_up, shared_down, side_in, side_out, side_gate.reshape(16, 128),
     )
 
 

time: 137 us -> 121 us (0.88)
  Pallas kernels: 131 us -> 120 us
  local copies, waits for them, and re-layouts: 5.08 us -> 0.82 us
    pallas_call x1, Pallas kernels: 131 us -> 120 us  [body(): pl.pallas_call(kernel, out_shape=pltpu.VMEM((TOK, D), bf16), in_specs=[in...]
    unnamed x17 -> x1, local copies, waits for them, and re-layouts: 2.88 us -> 0.82 us
where the time goes in v3:
time: 121 us
  Pallas kernels  120 us (99%)
    pallas_call x1, Pallas kernels, body(): pl.pallas_call(kernel, out_shape=pltpu.VMEM((TOK, D), bf16), in_specs=[in...  120 us

profile of v3, /device:TPU:1, one launch (start us, length us, event | category | flops | bytes accessed | tf_op | source)
XLA Modules:
  0.0 121.0 jit_solution(4712653142266580449)
XLA Ops:
  0.0 120.2 %routed_layer.1 = bf16[144,2048]{1,0:T(8,128)(2,1)S(1)} custom-call(bf16[144,2048]{1,0:T(8,128)(2,1)} %tok_hbm.1, f32[1,2048]{1,0:T(1,128)} %bitcast.10, s32[8,144]{1,0:T(8,128)} %bitcast.11, f32[8,144]{1,0:T(8,128)} %bitcast.12, bf16[128,2048]{1,0:T(8,128)(2,1)} %bitcast.7, bf16[128,2048]{1,0:T(8,128)(2,1)} %bitcast.8, bf16[128,2048]{1,0:T(8,128)(2,1)} %bitcast.9, ...), custom_call_target="tpu_custom_call" | custom-call | tf_op jit(solution)/shard_map/routed_layer/pallas_call | solution.py:545
  120.2 0.8 copy.15

commit v4 on v3

--- a/solution.py
+++ b/solution.py
@@ -12,6 +12,7 @@
 D = 2048
 HALF = 1024
 SUB = 512
+QUARTER = 256
 GROUP = 4
 ROWS = GROUP * TOK
 
@@ -22,23 +23,25 @@
     (1, 0), (0, 1), (0, 3), (0, 0),
 ]
 GROUPS = [12, 8, 4, 0]
-PARTS = {"g3a": (0, 2), "g3b": (2, 2), "g2a": (4, 2), "g2b": (6, 2), "g1": (8, 4), "g0": (12, 4)}
+PARTS = {"g2b": (6, 2), "g1": (8, 4), "g2a": (4, 2), "g0a": (12, 2), "g3a": (0, 2), "g0b": (14, 2), "g3b": (2, 2)}
 SUM_ORDER = [
-    ("C", "g2b"), ("relay", 1, 0, 0), ("relay", 0, 0, 1), ("relay", 1, 0, 1), ("relay", 0, 0, 0), ("C", "g1"),
-    ("free", 0, 3, 0), ("free", 1, 3, 0), ("free", 0, 0, 1), ("free", 0, 1, 0), ("free", 0, 1, 1), ("free", 1, 1, 0),
-    ("free", 1, 1, 1), ("C", "g0"), ("free", 0, 0, 0), ("free", 1, 0, 0), ("free", 1, 0, 1), ("pass", 0, 0, 1),
-    ("pass", 1, 0, 1), ("pass", 1, 0, 0), ("pass", 0, 0, 0), ("C", "g2a"), ("free", 0, 2, 1), ("relay", 1, 3, 0),
-    ("relay", 1, 3, 1), ("free", 1, 3, 1), ("free", 0, 3, 1), ("C", "x"), ("C", "y"), ("C", "g3a"),
-    ("relay", 0, 2, 0), ("relay", 0, 2, 1), ("relay", 1, 2, 0), ("relay", 1, 2, 1), ("free", 0, 2, 0),
-    ("relay", 1, 1, 1), ("relay", 1, 1, 0), ("C", "g3b"), ("relay", 0, 3, 0), ("relay", 0, 3, 1), ("free", 1, 2, 0),
-    ("free", 1, 2, 1), ("collect", 0, 0, 0), ("relay", 0, 1, 1), ("relay", 0, 1, 0), ("collect", 1, 0, 0),
-    ("S", "near"), ("pass", 1, 3, 1), ("pass", 1, 3, 0), ("pass", 0, 2, 0), ("pass", 1, 2, 0), ("pass", 0, 2, 1),
-    ("pass", 1, 2, 1), ("pass", 0, 3, 1), ("pass", 1, 1, 0), ("pass", 1, 1, 1), ("pass", 0, 3, 0), ("pass", 0, 1, 1),
-    ("S", "far"), ("pass", 0, 1, 0), ("collect", 1, 3, 0), ("free2", 1, 0, 1), ("S", "work"), ("collect", 0, 2, 0),
-    ("relay2", 0, 0, 0), ("relay2", 0, 0, 1), ("collect", 1, 2, 0), ("relay2", 1, 0, 0), ("relay2", 1, 0, 1),
-    ("collect", 0, 3, 0), ("free2", 0, 0, 1), ("collect", 1, 1, 0), ("free2", 1, 0, 0), ("collect", 0, 1, 0),
-    ("free2", 0, 0, 0), ("pass2", 0, 0, 0), ("pass2", 0, 0, 1), ("pass2", 1, 0, 0), ("pass2", 1, 0, 1),
-    ("final", 0, 0, 0), ("final", 1, 0, 0),
+    ("C", "g2b"), ("relay", 0, 0, 1), ("relay", 0, 0, 0), ("relay", 1, 0, 0), ("relay", 1, 0, 1), ("C", "g1"),
+    ("free", 0, 3, 0), ("free", 0, 1, 1), ("free", 1, 1, 1), ("free", 1, 1, 0), ("free", 1, 3, 0), ("free", 0, 1, 0),
+    ("free", 0, 0, 1), ("C", "g2a"), ("relay", 1, 3, 0), ("free", 0, 2, 1), ("relay", 1, 3, 1), ("free", 0, 3, 1),
+    ("free", 1, 3, 1), ("pass", 0, 0, 1), ("U", 0, 2), ("C", "g0a"), ("free", 1, 0, 0), ("free", 0, 0, 0),
+    ("pass", 0, 0, 0), ("pass", 1, 0, 0), ("U", 2, 1), ("pass", 1, 3, 1), ("U", 3, 1), ("C", "g3a"),
+    ("free", 0, 2, 0), ("relay", 1, 2, 0), ("relay", 0, 2, 0), ("relay", 0, 2, 1), ("relay", 1, 2, 1),
+    ("relay", 1, 1, 1), ("relay", 1, 1, 0), ("pass", 1, 3, 0), ("C", "g0b"), ("pass", 1, 0, 1), ("free", 1, 0, 1),
+    ("C", "g3b"), ("free", 1, 2, 0), ("relay", 0, 1, 0), ("free", 1, 2, 1), ("relay", 0, 1, 1), ("relay", 0, 3, 0),
+    ("relay", 0, 3, 1), ("collect", 0, 0, 0), ("pass", 1, 2, 1), ("S", "near"), ("pass", 0, 2, 1), ("pass", 1, 2, 0),
+    ("pass", 0, 2, 0), ("pass", 1, 1, 1), ("pass", 0, 1, 1), ("pass", 1, 1, 0), ("pass", 0, 1, 0), ("pass", 0, 3, 1),
+    ("collect", 1, 3, 0), ("free2", 1, 0, 1), ("pass", 0, 3, 0), ("S", "far"), ("collect", 1, 0, 0), ("S", "work"),
+    ("collect", 0, 2, 0), ("relay2", 0, 0, 0), ("relay2", 0, 1, 0), ("relay2", 0, 0, 1), ("relay2", 0, 1, 1),
+    ("collect", 1, 2, 0), ("relay2", 1, 0, 0), ("relay2", 1, 1, 0), ("relay2", 1, 0, 1), ("relay2", 1, 1, 1),
+    ("collect", 0, 1, 0), ("free2", 0, 0, 0), ("collect", 0, 3, 0), ("free2", 0, 0, 1), ("collect", 1, 1, 0),
+    ("free2", 1, 0, 0), ("pass2", 0, 0, 0), ("pass2", 0, 0, 1), ("pass2", 1, 0, 0), ("pass2", 0, 1, 0),
+    ("pass2", 0, 1, 1), ("pass2", 1, 1, 0), ("pass2", 1, 0, 1), ("pass2", 1, 1, 1), ("final", 0, 0, 0),
+    ("final", 1, 0, 0),
 ]
 SLOT = {place: i for i, place in enumerate(ORDER)}
 DY = [0, 1, 3, 2]
@@ -51,11 +54,11 @@
     side_in_hbm, side_out_hbm, sgate_hbm,
     out_ref,
     tok_ref, gain_ref, ids_ref, route_ref, side_ref, sgate_ref, in_sem,
-    xs, own, wg, wu, wd, wx, wdx, sb, sp, sg, su, sd, shid, sout, hid, rl, rf, rl2, rf2, w8, wrow, wpat,
+    xs, own, wg, wu, wd, wx, wdx, sb, sp, sg, su, sd, shid, sout, hid, early, rl, rf, rl2, rf2, w8, wrow, wpat,
     ag_send, ag_m1, ag_f1, ag_m2, ag_f2,
-    w_send, w_recv, w_fsend, w_frecv, w_dsend, w_drecv, w_loc, late_send, late_recv,
+    w_send, w_recv, w_frecv, w_drecv, w_loc, late_recv,
     x_send, x_recv, sb_dsend, sb_drecv,
-    s_send, s_recv, s_fsend, s_frecv, s_dsend, s_drecv, s_loc,
+    s_send, s_recv, s_frecv, s_drecv, s_loc,
     rs_send, rl_sem, rf_sem, rl2_sem, rf2_sem,
 ):
     ep = lax.axis_index("ep")
@@ -141,25 +144,25 @@
     w_p, w_m, w_fp, w_fm, w_d, w_l = [], [], [], [], {}, []
     for i, (src, dst) in enumerate(big):
         if i < 2:
-            w_p.append(remote(src, dst.at[2 * DYI[3]], w_send.at[i, 0], w_recv.at[i, 0], at_y(1)))
-            w_m.append(remote(src, dst.at[2 * DYI[1]], w_send.at[i, 1], w_recv.at[i, 1], at_y(3)))
+            w_p.append(remote(src, dst.at[2 * DYI[3]], w_send.at[i], w_recv.at[i, 0], at_y(1)))
+            w_m.append(remote(src, dst.at[2 * DYI[1]], w_send.at[i], w_recv.at[i, 1], at_y(3)))
         w_fp.append(remote(
             dst.at[2 * DYI[3], pl.ds(0, 64)], dst.at[2 * DYI[2], pl.ds(0, 64)],
-            w_fsend.at[i, 0], w_frecv.at[i, 0], at_y(1)))
+            w_send.at[i], w_frecv.at[i], at_y(1)))
         w_fm.append(remote(
             dst.at[2 * DYI[1], pl.ds(64, 64)], dst.at[2 * DYI[2], pl.ds(64, 64)],
-            w_fsend.at[i, 1], w_frecv.at[i, 1], at_y(3)))
+            w_send.at[i], w_frecv.at[i], at_y(3)))
         for dy in DY:
             w_d[i, dy] = remote(
                 src if dy == 0 else dst.at[2 * DYI[dy]], dst.at[2 * DYI[dy] + 1],
-                w_dsend.at[i, dy], w_drecv.at[i, dy], partner)
+                w_send.at[i], w_drecv.at[i, dy], partner)
         w_l.append(pltpu.make_async_copy(src, dst.at[0], w_loc.at[i]))
     first_rows, last_rows = pl.ds(0, 64), pl.ds(64, 64)
     late_p = [
-        remote(down_hbm.at[r], wd.at[2 * DYI[3], r], late_send.at[i, 0], late_recv.at[i, 0], at_y(1))
+        remote(down_hbm.at[r], wd.at[2 * DYI[3], r], w_send.at[2], late_recv.at[i, 0], at_y(1))
         for i, r in enumerate((first_rows, last_rows))]
     late_m = [
-        remote(down_hbm.at[r], wd.at[2 * DYI[1], r], late_send.at[i, 1], late_recv.at[i, 1], at_y(3))
+        remote(down_hbm.at[r], wd.at[2 * DYI[1], r], w_send.at[2], late_recv.at[i, 1], at_y(3))
         for i, r in enumerate((last_rows, first_rows))]
     for i in range(2):
         w_p[i].start()
@@ -191,10 +194,10 @@
                 xs.at[h, s(d, 0)], xs.at[h, s(d, 1)], ag_send.at[h], ag_m2.at[h, d, 1], along(a2, 3))
             f2[h, d, 0] = remote(
                 xs.at[h, s(d, 3), :, lo], xs.at[h, s(d, 2), :, lo],
-                ag_send.at[h], ag_f2.at[h, d, 0], along(a2, 1))
+                ag_send.at[h], ag_f2.at[h, d], along(a2, 1))
             f2[h, d, 1] = remote(
                 xs.at[h, s(d, 1), :, hi], xs.at[h, s(d, 2), :, hi],
-                ag_send.at[h], ag_f2.at[h, d, 1], along(a2, 3))
+                ag_send.at[h], ag_f2.at[h, d], along(a2, 3))
 
     both = [(h, k) for h in range(2) for k in range(2)]
     for h, k in both:
@@ -219,18 +222,18 @@
 
     s_p, s_m, s_fp, s_fm, s_d, s_l = [], [], [], [], {}, []
     for i, (src, dst) in enumerate([(sg_hbm, sg), (su_hbm, su), (sd_hbm, sd)]):
-        s_p.append(remote(src, dst.at[2 * DYI[3]], s_send.at[i, 0], s_recv.at[i, 0], at_y(1)))
-        s_m.append(remote(src, dst.at[2 * DYI[1]], s_send.at[i, 1], s_recv.at[i, 1], at_y(3)))
+        s_p.append(remote(src, dst.at[DYI[3]], s_send.at[i], s_recv.at[i, 0], at_y(1)))
+        s_m.append(remote(src, dst.at[DYI[1]], s_send.at[i], s_recv.at[i, 1], at_y(3)))
         s_fp.append(remote(
-            dst.at[2 * DYI[3], pl.ds(0, 32)], dst.at[2 * DYI[2], pl.ds(0, 32)],
-            s_fsend.at[i, 0], s_frecv.at[i, 0], at_y(1)))
+            dst.at[DYI[3], pl.ds(0, 32)], dst.at[DYI[2], pl.ds(0, 32)],
+            s_send.at[i], s_frecv.at[i], at_y(1)))
         s_fm.append(remote(
-            dst.at[2 * DYI[1], pl.ds(32, 32)], dst.at[2 * DYI[2], pl.ds(32, 32)],
-            s_fsend.at[i, 1], s_frecv.at[i, 1], at_y(3)))
+            dst.at[DYI[1], pl.ds(32, 32)], dst.at[DYI[2], pl.ds(32, 32)],
+            s_send.at[i], s_frecv.at[i], at_y(3)))
         for dy in DY:
             s_d[i, dy] = remote(
-                src if dy == 0 else dst.at[2 * DYI[dy]], dst.at[2 * DYI[dy] + 1],
-                s_dsend.at[i, dy], s_drecv.at[i, dy], partner)
+                src if dy == 0 else dst.at[DYI[dy]], dst.at[4 + DYI[dy]],
+                s_send.at[i], s_drecv.at[i], partner)
         s_l.append(pltpu.make_async_copy(src, dst.at[0], s_loc.at[i]))
 
     def silu(v):
@@ -291,14 +294,14 @@
                 s_d[i, 1].start()
         elif part == "far":
             for i in range(3):
-                s_fp[i].wait_recv()
-                s_fm[i].wait_recv()
+                far = (sg, su, sd)[i].at[DYI[2]]
+                pltpu.make_async_copy(far, far, s_frecv.at[i]).wait()
                 s_d[i, 2].start()
         else:
             for i in range(3):
                 s_l[i].wait()
-                for dy in DY:
-                    s_d[i, dy].wait_recv()
+                across = (sg, su, sd)[i].at[pl.ds(4, 4)]
+                pltpu.make_async_copy(across, across, s_drecv.at[i]).wait()
             shared_expert()
 
     def down(base, count):
@@ -314,6 +317,30 @@
 
         lax.fori_loop(0, 4, step, 0)
 
+    def down_early(base):
+        def step(n, carry):
+            cols = pl.ds(pl.multiple_of(n * SUB, SUB), SUB)
+            rows = hid[pl.ds(base, 2)].reshape(2 * TOK, 1152)
+            part = jnp.dot(
+                rows[:, :768], wd[pl.ds(0, 6), :, cols].reshape(768, SUB), preferred_element_type=f32)
+            early[:, cols] = part + jnp.dot(rows[:, 1024:], wdx[:, cols], preferred_element_type=f32)
+            return carry
+
+        lax.fori_loop(0, 4, step, 0)
+
+    def down_late(base):
+        def step(n, carry):
+            h = n // 2
+            cols = pl.ds(pl.multiple_of(n * SUB, SUB), SUB)
+            to = pl.ds(pl.multiple_of((n % 2) * SUB, SUB), SUB)
+            rows = hid[pl.ds(base, 2)].reshape(2 * TOK, 1152)
+            part = early[:, cols] + jnp.dot(
+                rows[:, 768:1024], wd[pl.ds(6, 2), :, cols].reshape(256, SUB), preferred_element_type=f32)
+            xs[h, pl.ds(base, 2), :, to] = part.astype(jnp.bfloat16).reshape(2, TOK, SUB)
+            return carry
+
+        lax.fori_loop(0, 4, step, 0)
+
     for h, k in both:
         m1[h, k].wait_recv()
         f1[h, k].start()
@@ -330,9 +357,14 @@
         w_fm[i].start()
         w_d[i, 1].start()
 
+    def far_rows(d):
+        for h in range(2):
+            here = xs.at[h, src_slot(h, d, 2)]
+            pltpu.make_async_copy(here, here, ag_f2.at[h, d]).wait()
+
     def weights_far(i):
-        w_fp[i].wait_recv()
-        w_fm[i].wait_recv()
+        far = (wg, wu, wd)[i].at[2 * DYI[2]]
+        pltpu.make_async_copy(far, far, w_frecv.at[i]).wait()
         w_d[i, 2].start()
 
     weights_on(0)
@@ -384,8 +416,7 @@
     weights_far(0)
     hidden(GROUPS[1], 0, 3)
     weights_far(1)
-    for h, k in both:
-        f2[h, 0, k].wait_recv()
+    far_rows(0)
     for i in range(2):
         w_d[i, 2].wait_recv()
     hidden(GROUPS[0], 3, 1)
@@ -404,31 +435,24 @@
         m2[h, 2, k].wait_recv()
         f2[h, 2, k].start()
     dense_hidden(GROUPS[1])
-    for h, k in both:
-        f2[h, 3, k].wait_recv()
+    far_rows(3)
+    hidden(GROUPS[2], 0, 2)
     late_p[1].wait_recv()
     w_d[2, 3].start()
     late_m[1].wait_recv()
     w_d[2, 1].start()
-    hidden(GROUPS[2], 0, 4)
+    hidden(GROUPS[2], 2, 2)
+    dense_hidden(GROUPS[2])
     weights_far(2)
-    dense_hidden(GROUPS[2])
-    for d in (1, 2):
-        for h, k in both:
-            f2[h, d, k].wait_recv()
+    w_l[2].wait()
+    for dy in (0, 1, 3):
+        w_d[2, dy].wait_recv()
+    down_early(PARTS["g2b"][0])
+    far_rows(1)
+    far_rows(2)
     for h in range(2):
         pltpu.make_async_copy(xs.at[h, pl.ds(0, 15)], xs.at[h, pl.ds(0, 15)], ag_send.at[h]).wait()
-
-    w_l[2].wait()
-    for dy in DY:
-        w_d[2, dy].wait_recv()
-
-    def last_hidden(part):
-        if part == "x":
-            hidden(GROUPS[3], 0, 2)
-        else:
-            hidden(GROUPS[3], 2, 2)
-            dense_hidden(GROUPS[3])
+    w_d[2, 2].wait_recv()
 
     rs_axes = [("z", "x"), ("x", "z")]
 
@@ -449,19 +473,22 @@
                     xs.at[h, t(2, q), :, sum_cols], rl.at[h, q, k], rs_send.at[h], rl_sem.at[h, q, k], to)
                 s1[h, q, k] = remote(
                     xs.at[h, t(near, q), :, sum_cols], rf.at[h, q, k, :, sum_cols],
-                    rs_send.at[h], rf_sem.at[h, q, k, 0], to)
+                    rs_send.at[h], rf_sem.at[h, q], to)
                 e1[h, q, k] = remote(
                     xs.at[h, t(near, q), :, own_cols], rf.at[h, q, k, :, own_cols],
-                    rs_send.at[h], rf_sem.at[h, q, k, 1], to)
+                    rs_send.at[h], rf_sem.at[h, q], to)
             to = along(b2, step)
-            r2[h, k] = remote(
-                xs.at[h, t(0, 2), :, sum_cols], rl2.at[h, k], rs_send.at[h], rl2_sem.at[h, k], to)
-            s2[h, k] = remote(
-                xs.at[h, t(0, near), :, sum_cols], rf2.at[h, k, :, sum_cols],
-                rs_send.at[h], rf2_sem.at[h, k, 0], to)
+            for p in range(2):
+                cols = pl.ds(SUB * k + QUARTER * p, QUARTER)
+                r2[h, p, k] = remote(
+                    xs.at[h, t(0, 2), :, cols], rl2.at[h, k, :, pl.ds(QUARTER * p, QUARTER)],
+                    rs_send.at[h], rl2_sem.at[h, p, k], to)
+                s2[h, p, k] = remote(
+                    xs.at[h, t(0, near), :, cols], rf2.at[h, k, :, cols],
+                    rs_send.at[h], rf2_sem.at[h, k, p], to)
             e2[h, k] = remote(
                 xs.at[h, t(0, near), :, own_cols], rf2.at[h, k, :, own_cols],
-                rs_send.at[h], rf2_sem.at[h, k, 1], to)
+                rs_send.at[h], rf2_sem.at[h, k, 2], to)
 
     def add(slot, h, cols, *more):
         total = xs[h, slot, :, cols].astype(f32)
@@ -472,10 +499,15 @@
     for op in SUM_ORDER:
         name = op[0]
         if name == "C":
-            if op[1] in PARTS:
+            if op[1] == "g2b":
+                down_late(PARTS["g2b"][0])
+            else:
                 down(*PARTS[op[1]])
-            else:
-                last_hidden(op[1])
+            continue
+        if name == "U":
+            hidden(GROUPS[3], op[1], op[2])
+            if op[1] + op[2] == 4:
+                dense_hidden(GROUPS[3])
             continue
         if name == "S":
             shared_step(op[1])
@@ -491,43 +523,33 @@
             add(dst_slot(h, near, q), h, halves[k], rl[h, q, k])
             s1[h, q, k].start()
         elif name == "collect":
-            for i in range(2):
-                e1[h, q, i].wait_recv()
-                s1[h, q, i].wait_recv()
+            pltpu.make_async_copy(rf.at[h, q], rf.at[h, q], rf_sem.at[h, q]).wait()
             add(dst_slot(h, 0, q), h, pl.ds(0, HALF), rf[h, q, 0], rf[h, q, 1])
         elif name == "relay2":
-            r2[h, k].start()
+            r2[h, q, k].start()
         elif name == "free2":
             e2[h, k].start()
         elif name == "pass2":
-            r2[h, k].wait_recv()
-            add(dst_slot(h, 0, near), h, halves[k], rl2[h, k])
-            s2[h, k].start()
+            r2[h, q, k].wait_recv()
+            add(
+                dst_slot(h, 0, near), h, pl.ds(SUB * k + QUARTER * q, QUARTER),
+                rl2[h, k, :, pl.ds(QUARTER * q, QUARTER)])
+            s2[h, q, k].start()
         else:
             for i in range(2):
                 e2[h, i].wait_recv()
-                s2[h, i].wait_recv()
+                s2[h, 0, i].wait_recv()
+                s2[h, 1, i].wait_recv()
             total = xs[h, SLOT[0, 0]].astype(f32) + rf2[h, 0].astype(f32) + rf2[h, 1].astype(f32)
             total = total + sout[:, pl.ds(h * HALF, HALF)]
             out_ref[:, pl.ds(h * HALF, HALF)] = total.astype(jnp.bfloat16)
 
     for h in range(2):
         pltpu.make_async_copy(xs.at[h, pl.ds(0, 15)], xs.at[h, pl.ds(0, 15)], rs_send.at[h]).wait()
-    for i in range(2):
-        w_p[i].wait_send()
-        w_m[i].wait_send()
-        late_p[i].wait_send()
-        late_m[i].wait_send()
-    for i in range(3):
-        w_fp[i].wait_send()
-        w_fm[i].wait_send()
-        s_p[i].wait_send()
-        s_m[i].wait_send()
-        s_fp[i].wait_send()
-        s_fm[i].wait_send()
-        for dy in DY:
-            w_d[i, dy].wait_send()
-            s_d[i, dy].wait_send()
+    for sent, sem in ((wg, w_send.at[0]), (wu, w_send.at[1]), (wd, w_send.at[2])):
+        pltpu.make_async_copy(sent.at[pl.ds(0, 7)], sent.at[pl.ds(0, 7)], sem).wait()
+    for i, sent in enumerate((sg, su, sd)):
+        pltpu.make_async_copy(sent.at[pl.ds(0, 7)], sent.at[pl.ds(0, 7)], s_send.at[i]).wait()
     pltpu.make_async_copy(wrow.at[pl.ds(0, 15)], wrow.at[pl.ds(0, 15)], x_send.at[0]).wait()
     pltpu.make_async_copy(
         sb.at[0, :, pl.ds(0, 1920)], sb.at[0, :, pl.ds(0, 1920)], x_send.at[1]).wait()
@@ -570,6 +592,7 @@
             vmem((TOK, 512), bf16),
             vmem((TOK, D), f32),
             vmem((16, TOK, 1152), bf16),
+            vmem((2 * TOK, D), f32),
             vmem((2, 4, 2, TOK, SUB), bf16),
             vmem((2, 4, 2, TOK, HALF), bf16),
             vmem((2, 2, TOK, SUB), bf16),
@@ -577,11 +600,11 @@
             vmem((16, 8, 128), f32),
             vmem((16, 8, 128), f32),
             vmem((16, TOK, 128), f32),
-            dma((2,)), dma((2, 2)), dma((2, 2)), dma((2, 4, 2)), dma((2, 4, 2)),
-            dma((2, 2)), dma((2, 2)), dma((3, 2)), dma((3, 2)), dma((3, 4)), dma((3, 4)), dma((3,)),
-            dma((2, 2)), dma((2, 2)), dma((2,)), dma((2,)), dma(()), dma(()),
-            dma((3, 2)), dma((3, 2)), dma((3, 2)), dma((3, 2)), dma((3, 4)), dma((3, 4)), dma((3,)),
-            dma((2,)), dma((2, 4, 2)), dma((2, 4, 2, 2)), dma((2, 2)), dma((2, 2, 2)),
+            dma((2,)), dma((2, 2)), dma((2, 2)), dma((2, 4, 2)), dma((2, 4)),
+            dma((3,)), dma((2, 2)), dma((3,)), dma((3, 4)), dma((3,)), dma((2, 2)),
+            dma((2,)), dma((2,)), dma(()), dma(()),
+            dma((3,)), dma((3, 2)), dma((3,)), dma((3,)), dma((3,)),
+            dma((2,)), dma((2, 4, 2)), dma((2, 4)), dma((2, 2, 2)), dma((2, 2, 3)),
         ],
         compiler_params=pltpu.CompilerParams(
             collective_id=0, has_side_effects=True, vmem_limit_bytes=60 * 1024 * 1024),

time: 121 us -> 119 us (0.983)
  Pallas kernels: 120 us -> 118 us
    pallas_call x1, Pallas kernels: 120 us -> 118 us  [body(): pl.pallas_call(kernel, out_shape=pltpu.VMEM((TOK, D), bf16), in_specs=[in...]
where the time goes in v4:
time: 119 us
  Pallas kernels  118 us (99%)
    pallas_call x1, Pallas kernels, body(): pl.pallas_call(kernel, out_shape=pltpu.VMEM((TOK, D), bf16), in_specs=[in...  118 us

profile of v4, /device:TPU:1, one launch (start us, length us, event | category | flops | bytes accessed | tf_op | source)
XLA Modules:
  0.0 119.2 jit_solution(10346755086828015445)
XLA Ops:
  0.0 118.4 %routed_layer.1 = bf16[144,2048]{1,0:T(8,128)(2,1)S(1)} custom-call(bf16[144,2048]{1,0:T(8,128)(2,1)} %tok_hbm.1, f32[1,2048]{1,0:T(1,128)} %bitcast.10, s32[8,144]{1,0:T(8,128)} %bitcast.11, f32[8,144]{1,0:T(8,128)} %bitcast.12, bf16[128,2048]{1,0:T(8,128)(2,1)} %bitcast.7, bf16[128,2048]{1,0:T(8,128)(2,1)} %bitcast.8, bf16[128,2048]{1,0:T(8,128)(2,1)} %bitcast.9, ...), custom_call_target="tpu_custom_call" | custom-call | tf_op jit(solution)/shard_map/routed_layer/pallas_call | solution.py:567
  118.4 0.8 copy.15

commit v5 on v4

--- a/solution.py
+++ b/solution.py
@@ -29,10 +29,10 @@
     ("free", 0, 3, 0), ("free", 0, 1, 1), ("free", 1, 1, 1), ("free", 1, 1, 0), ("free", 1, 3, 0), ("free", 0, 1, 0),
     ("free", 0, 0, 1), ("C", "g2a"), ("relay", 1, 3, 0), ("free", 0, 2, 1), ("relay", 1, 3, 1), ("free", 0, 3, 1),
     ("free", 1, 3, 1), ("pass", 0, 0, 1), ("U", 0, 2), ("C", "g0a"), ("free", 1, 0, 0), ("free", 0, 0, 0),
-    ("pass", 0, 0, 0), ("pass", 1, 0, 0), ("U", 2, 1), ("pass", 1, 3, 1), ("U", 3, 1), ("C", "g3a"),
-    ("free", 0, 2, 0), ("relay", 1, 2, 0), ("relay", 0, 2, 0), ("relay", 0, 2, 1), ("relay", 1, 2, 1),
-    ("relay", 1, 1, 1), ("relay", 1, 1, 0), ("pass", 1, 3, 0), ("C", "g0b"), ("pass", 1, 0, 1), ("free", 1, 0, 1),
-    ("C", "g3b"), ("free", 1, 2, 0), ("relay", 0, 1, 0), ("free", 1, 2, 1), ("relay", 0, 1, 1), ("relay", 0, 3, 0),
+    ("pass", 0, 0, 0), ("pass", 1, 0, 0), ("U", 2, 2), ("pass", 1, 3, 1), ("C", "g3a"), ("free", 0, 2, 0),
+    ("relay", 1, 2, 0), ("relay", 0, 2, 0), ("relay", 0, 2, 1), ("relay", 1, 2, 1), ("relay", 1, 1, 1),
+    ("relay", 1, 1, 0), ("pass", 1, 3, 0), ("C", "g0b"), ("pass", 1, 0, 1), ("free", 1, 0, 1), ("C", "g3b"),
+    ("free", 1, 2, 0), ("relay", 0, 1, 0), ("free", 1, 2, 1), ("relay", 0, 1, 1), ("relay", 0, 3, 0),
     ("relay", 0, 3, 1), ("collect", 0, 0, 0), ("pass", 1, 2, 1), ("S", "near"), ("pass", 0, 2, 1), ("pass", 1, 2, 0),
     ("pass", 0, 2, 0), ("pass", 1, 1, 1), ("pass", 0, 1, 1), ("pass", 1, 1, 0), ("pass", 0, 1, 0), ("pass", 0, 3, 1),
     ("collect", 1, 3, 0), ("free2", 1, 0, 1), ("pass", 0, 3, 0), ("S", "far"), ("collect", 1, 0, 0), ("S", "work"),

time: 119 us -> 118 us (level)
  no operation moved by 1% of the time
where the time goes in v5:
time: 118 us
  Pallas kernels  118 us (100%)
    pallas_call x1, Pallas kernels, body(): pl.pallas_call(kernel, out_shape=pltpu.VMEM((TOK, D), bf16), in_specs=[in...  118 us

profile of v5, /device:TPU:1, one launch (start us, length us, event | category | flops | bytes accessed | tf_op | source)
XLA Modules:
  0.0 118.3 jit_solution(13409293211274722440)
XLA Ops:
  0.0 117.5 %routed_layer.1 = bf16[144,2048]{1,0:T(8,128)(2,1)S(1)} custom-call(bf16[144,2048]{1,0:T(8,128)(2,1)} %tok_hbm.1, f32[1,2048]{1,0:T(1,128)} %bitcast.10, s32[8,144]{1,0:T(8,128)} %bitcast.11, f32[8,144]{1,0:T(8,128)} %bitcast.12, bf16[128,2048]{1,0:T(8,128)(2,1)} %bitcast.7, bf16[128,2048]{1,0:T(8,128)(2,1)} %bitcast.8, bf16[128,2048]{1,0:T(8,128)(2,1)} %bitcast.9, ...), custom_call_target="tpu_custom_call" | custom-call | tf_op jit(solution)/shard_map/routed_layer/pallas_call | solution.py:567
  117.5 0.8 copy.15
